TPU v7x, 32 devices: a whole 2x2x4 slice. The times are simulated.
32 devices in a mesh: kv: 8 (over z, y), tp: 4 (over x, core).
Axes of the slice: x: 2, y: 2, z: 4, core: 2. Of those that a mesh axis runs over, the one named last changes fastest.
Arguments:
- tokens: bfloat16 [64, 4096], P(None, 'kv'), may hold values from -170 to 170
- mix_gain: float32 [4096], P('kv'), may hold values from 0.1 to 1.9
- w_query: bfloat16 [4096, 2048], P('kv', 'tp'), may hold values from -0.09375 to 0.09375
- w_key: bfloat16 [4096, 512], P('kv', 'tp'), may hold values from -0.09375 to 0.09375
- w_value: bfloat16 [4096, 512], P('kv', 'tp'), may hold values from -0.09375 to 0.09375
- w_forget: bfloat16 [4096, 32], P('kv', 'tp'), may hold values from -0.09375 to 0.09375
- query_gain: float32 [64], replicated, may hold values from 0.1 to 1.9
- key_cache: bfloat16 [64, 8, 64, 8192], P(None, 'tp', None, 'kv'), may hold values from -1300 to 1300
- value_cache: bfloat16 [64, 8, 64, 8192], P(None, 'tp', None, 'kv'), may hold values from -8 to 8
- decay_cache: float32 [64, 32, 8192], P(None, 'tp', 'kv'), may hold values from -1066.96 to 0, as said below
- w_out: bfloat16 [2048, 4096], P('tp', 'kv'), may hold values from -1 to 1
- mlp_gain: float32 [4096], P('kv'), may hold values from 0.1 to 1.9
- w_up: bfloat16 [4096, 16384], P('kv', 'tp'), may hold values from -0.09375 to 0.09375
- w_down: bfloat16 [16384, 4096], P('tp', 'kv'), may hold values from -0.046875 to 0.046875
Outputs:
- layer_out: bfloat16 [64, 4096], P(None, 'kv')
Inputs may be any that keep to these rules, and one draw needn't show every extreme that they name: `decay_cache`: each entry is the sum of the non-positive log forget gates of the later cached positions of its sequence and head: 0 at the last cached position, never smaller at a later position.
All inputs are finite; a program needn't handle non-finite values.
Results may differ from a plain program's by a relative error of at most 0.015.
Values may be sent and summed in bfloat16 or wider, within the bound.
A program may use at most 128 MiB of HBM per device.

v0:
```python
import functools

import jax
import jax.numpy as jnp
from jax import lax
from jax.experimental import pallas as pl
from jax.experimental.pallas import tpu as pltpu
from jax.sharding import PartitionSpec as P

MESH = pl.DeviceIdType.MESH
HEAD_DIM = 64
EPS = 1e-06
F32 = jnp.float32
BF16 = jnp.bfloat16


def greet(n, t, with_tp):
    kv, tp = lax.axis_index("kv"), lax.axis_index("tp")
    barrier = pltpu.get_barrier_semaphore()
    count = n - 1
    for i in range(1, n):
        pl.semaphore_signal(
            barrier, inc=1, device_id=(lax.rem(kv + i, n), tp), device_id_type=MESH
        )
    if with_tp:
        count += t - 1
        for i in range(1, t):
            pl.semaphore_signal(
                barrier, inc=1, device_id=(kv, lax.rem(tp + i, t)), device_id_type=MESH
            )
    pl.semaphore_wait(barrier, count)


def remote(src, dst, send, recv, kv, tp):
    return pltpu.make_async_remote_copy(
        src_ref=src,
        dst_ref=dst,
        send_sem=send,
        recv_sem=recv,
        device_id=(kv, tp),
        device_id_type=MESH,
    )


def project_kernel(
    n, t, d, tok, gain, wq, wk, wv, wf, qgain, out, parts, got, mine, ssem, rsem, asem, bsem
):
    kv, tp = lax.axis_index("kv"), lax.axis_index("tp")
    greet(n, t, False)
    rows = tok.shape[0]
    rc = rows // n
    nq, nk, nf = wq.shape[1], wk.shape[1], wf.shape[0]
    stream = tok[...].astype(F32)
    squares = jnp.sum(stream * stream, axis=1, keepdims=True)
    normed = (stream * gain[...]).astype(BF16)
    q = jnp.dot(normed, wq[...], preferred_element_type=F32)
    k = jnp.dot(normed, wk[...], preferred_element_type=F32)
    v = jnp.dot(normed, wv[...], preferred_element_type=F32)
    f = lax.dot_general(
        normed, wf[...], (((1,), (1,)), ((), ())), preferred_element_type=F32
    )
    for p in range(n):
        cut = slice(p * rc, (p + 1) * rc)
        parts[p, :, 0:nq] = q[cut]
        parts[p, :, nq : nq + nk] = k[cut]
        parts[p, :, nq + nk : nq + 2 * nk] = v[cut]
        base = nq + 2 * nk
        parts[p, :, base : base + 128] = jnp.broadcast_to(squares[cut], (rc, 128))
        parts[p, :, base : base + nf] = f[cut]
    sends = []
    for i in range(1, n):
        peer = lax.rem(kv + i, n)
        c = remote(parts.at[peer], got.at[i], ssem.at[i], rsem.at[i], peer, tp)
        c.start()
        sends.append(c)
    total = parts[kv]
    for c in sends:
        c.wait_recv()
    for i in range(1, n):
        total = total + got[i]
    base = nq + 2 * nk
    scale = lax.rsqrt(total[:, base + 127 : base + 128] / d + EPS)
    scaled = total * scale
    raw = scaled[:, 0:nq]
    raw2 = raw * raw
    head = lax.broadcasted_iota(jnp.int32, raw.shape, 1) // HEAD_DIM
    inverse = jnp.zeros_like(raw)
    for h in range(nq // HEAD_DIM):
        on = head == h
        mean = jnp.sum(jnp.where(on, raw2, 0.0), axis=1, keepdims=True) / HEAD_DIM
        inverse = jnp.where(on, lax.rsqrt(mean + EPS), inverse)
    gains = jnp.concatenate([qgain[...]] * (nq // HEAD_DIM), axis=1)
    mine[:, 0:nq] = raw * inverse * gains
    mine[:, nq:base] = scaled[:, nq:base]
    gate = scaled[:, base:]
    mine[:, base:] = jnp.minimum(gate, 0.0) - jnp.log1p(jnp.exp(-jnp.abs(gate)))
    gathers = []
    for i in range(1, n):
        peer = lax.rem(kv + i, n)
        c = remote(mine, out.at[kv], asem.at[i], bsem.at[i], peer, tp)
        c.start()
        gathers.append(c)
    out[kv] = mine[...]
    for i in range(1, n):
        gathers[i - 1].wait_recv()
    for c in sends + gathers:
        c.wait_send()


def attend_kernel(sharing, q_ref, k_ref, v_ref, d_ref, o_ref):
    steps, heads, _ = q_ref.shape
    groups = heads // sharing
    row = lax.broadcasted_iota(jnp.int32, (heads, HEAD_DIM), 0) // sharing
    scores = [
        jnp.dot(q_ref[i], k_ref[i], preferred_element_type=F32) * (HEAD_DIM**-0.5) + d_ref[i]
        for i in range(steps)
    ]
    peaks = [jnp.max(s, axis=1, keepdims=True) for s in scores]
    weights = [jnp.exp(s - m) for s, m in zip(scores, peaks)]
    sums = [jnp.sum(w, axis=1, keepdims=True) for w in weights]
    outs = [
        lax.dot_general(
            w.astype(BF16), v_ref[i], (((1,), (1,)), ((), ())), preferred_element_type=F32
        )
        for i, w in enumerate(weights)
    ]
    for i in range(steps):
        o = outs[i]
        picked = o[:, 0:HEAD_DIM]
        for g in range(1, groups):
            picked = jnp.where(row == g, o[:, g * HEAD_DIM : (g + 1) * HEAD_DIM], picked)
        o_ref[i, :, 0:64] = picked
        o_ref[i, :, 64:96] = jnp.broadcast_to(peaks[i], (heads, 32))
        o_ref[i, :, 96:128] = jnp.broadcast_to(sums[i], (heads, 32))


def rest_kernel(
    n, t, d, packed, own, tok, gain, wo_hbm, wu_hbm, wd_hbm, out,
    wo, wu, wd, got, att, allatt, full, tpa, tpb, upsend, upgot, upsend2, upgot2, keep, sqs, sqgot, hid,
    wsem, sem, tsem,
):
    kv, tp = lax.axis_index("kv"), lax.axis_index("tp")
    loads = [
        pltpu.make_async_copy(a, b, wsem.at[j])
        for j, (a, b) in enumerate(((wo_hbm, wo), (wu_hbm, wu), (wd_hbm, wd)))
    ]
    for c in loads:
        c.start()
    greet(n, t, True)
    rows, heads, _ = packed.shape
    rc = rows // n
    ffc = wu.shape[1] // n
    started = []

    def send(kind, i, src, dst, peer=None):
        if peer is None:
            peer = lax.rem(kv + i, n)
        c = remote(src(peer), dst, sem.at[2 * kind, i], sem.at[2 * kind + 1, i], peer, tp)
        c.start()
        started.append(c)
        return c

    def tp_sum(kind, buf, value):
        buf[tp] = value.astype(BF16)
        copies = []
        for i in range(1, t):
            c = remote(
                buf.at[tp], buf.at[tp], tsem.at[2 * kind, i], tsem.at[2 * kind + 1, i],
                kv, lax.rem(tp + i, t),
            )
            c.start()
            copies.append(c)
            started.append(c)
        for c in copies:
            c.wait_recv()
        total = buf[0].astype(F32)
        for j in range(1, t):
            total = total + buf[j].astype(F32)
        return total.astype(BF16).astype(F32)

    copies = [
        send(0, i, lambda p: packed.at[pl.ds(p * rc, rc)], got.at[i]) for i in range(1, n)
    ]
    mine = packed[pl.ds(kv * rc, rc)]
    extra = own[pl.ds(kv * rc, rc)]
    own_score = extra[:, :, 64:65]
    forget = extra[:, :, 96:97]
    for c in copies:
        c.wait_recv()
    blocks = [mine] + [got[i] for i in range(1, n)]
    peaks = [b[:, :, 64:65] + forget for b in blocks]
    peak = own_score
    for p in peaks:
        peak = jnp.maximum(peak, p)
    own_weight = jnp.exp(own_score - peak)
    mass = own_weight
    summed = own_weight.astype(BF16).astype(F32) * extra[:, :, 0:64]
    for b, p in zip(blocks, peaks):
        w = jnp.exp(p - peak)
        mass = mass + w * b[:, :, 96:97]
        summed = summed + w * b[:, :, 0:64]
    head = summed / mass
    for h in range(heads):
        att[:, h * HEAD_DIM : (h + 1) * HEAD_DIM] = head[:, h, :].astype(BF16)
    copies = [send(1, i, lambda p: att, allatt.at[kv]) for i in range(1, n)]
    allatt[kv] = att[...]
    loads[0].wait()
    for c in copies:
        c.wait_recv()
    for p in range(n):
        full[p * rc : (p + 1) * rc, :] = allatt[p].astype(F32)
    attn = jnp.dot(full[...].astype(BF16), wo[...], preferred_element_type=F32)
    attn = tp_sum(0, tpa, attn)
    residual = (tok[...].astype(F32) + attn).astype(BF16).astype(F32)
    normed = (residual * gain[...]).astype(BF16)
    loads[1].wait()
    half = n // 2
    side = lax.rem(kv, 2)
    place = kv // 2
    partner = kv + 1 - 2 * side
    order = list(range(1, half)) + [0]

    def term(dest):
        cols = pl.ds(pl.multiple_of(dest * ffc, ffc), ffc)
        return jnp.dot(normed, wu[:, cols], preferred_element_type=F32)

    firsts = {}
    for j in order:
        upsend[j] = term(2 * lax.rem(place + j, half) + 1 - side).astype(BF16)
        firsts[j] = send(2, j, lambda p: upsend.at[j], upgot.at[j], partner)
    for j in order:
        keep[j] = term(2 * lax.rem(place + j, half) + side)
    sqs[...] = lax.dot_general(
        jnp.ones((8, residual.shape[1]), F32),
        residual * residual,
        (((1,), (1,)), ((), ())),
        preferred_element_type=F32,
        precision=lax.Precision.HIGHEST,
    )
    sq_copies = [send(3, i, lambda p: sqs, sqgot.at[i]) for i in range(1, n)]
    seconds = {}
    for j in order:
        firsts[j].wait_recv()
        part = keep[j] + upgot[j].astype(F32)
        if j:
            upsend2[j] = part.astype(BF16)
            seconds[j] = send(
                4, j, lambda p: upsend2.at[j], upgot2.at[j], 2 * lax.rem(place + j, half) + side
            )
    total = sqs[...]
    for i in range(1, n):
        sq_copies[i - 1].wait_recv()
        total = total + sqgot[i]
    r = lax.broadcasted_iota(jnp.int32, (rows, rows), 0)
    c_ = lax.broadcasted_iota(jnp.int32, (rows, rows), 1)
    wide = jnp.broadcast_to(total[0:1, :], (rows, rows))
    column = jnp.sum(jnp.where(r == c_, wide, 0.0), axis=1, keepdims=True)
    scale = lax.rsqrt(column / d + EPS)
    for j in range(1, half):
        seconds[j].wait_recv()
        part = part + upgot2[j].astype(F32)
    hidden = jnp.square(jnp.maximum(part * scale, 0.0)).astype(BF16)
    hid[kv] = hidden
    across = {0: send(6, 0, lambda p: hid.at[kv], hid.at[kv], partner)}
    along = {}
    for j in range(1, half):
        along[j] = send(
            5, j, lambda p: hid.at[kv], hid.at[kv], 2 * lax.rem(place + j, half) + side
        )
    loads[2].wait()

    def lower(src):
        there = pl.ds(pl.multiple_of(src * ffc, ffc), ffc)
        return jnp.dot(hid[src], wd[there, :], preferred_element_type=F32)

    down = lower(kv)
    for j in range(1, half):
        src = 2 * lax.rem(place + half - j, half) + side
        along[j].wait_recv()
        across[j] = send(6, j, lambda p: hid.at[src], hid.at[src], partner)
        down = down + lower(src)
    for j in range(half):
        across[j].wait_recv()
        down = down + lower(2 * lax.rem(place + half - j, half) + 1 - side)
    mlp = tp_sum(1, tpb, down)
    out[...] = (residual + mlp).astype(BF16)
    for c in started:
        c.wait_send()


def shards(
    n, t, tokens, mix_gain, w_query, w_key, w_value, w_forget, query_gain,
    key_cache, value_cache, decay_cache, w_out, mlp_gain, w_up, w_down,
):
    rows, dl = tokens.shape
    d = dl * n
    rc = rows // n
    heads = w_forget.shape[1]
    groups = key_cache.shape[1]
    sharing = heads // groups
    nq, nk = w_query.shape[1], w_key.shape[1]
    span = key_cache.shape[3]
    vmem = pl.BlockSpec(memory_space=pltpu.VMEM)
    anywhere = pl.BlockSpec(memory_space=pl.ANY)
    nk_pad = nk
    width = nq + 2 * nk_pad + 128
    dma = pltpu.SemaphoreType.DMA
    proj = pl.pallas_call(
        functools.partial(project_kernel, n, t, d),
        out_shape=jax.ShapeDtypeStruct((n, rc, width), F32),
        in_specs=[vmem] * 7,
        out_specs=vmem,
        scratch_shapes=[
            pltpu.VMEM((n, rc, width), F32),
            pltpu.VMEM((n, rc, width), F32),
            pltpu.VMEM((rc, width), F32),
            dma((n,)), dma((n,)), dma((n,)), dma((n,)),
        ],
        compiler_params=pltpu.CompilerParams(collective_id=0, has_side_effects=True),
    )(
        tokens, mix_gain[None, :], w_query, w_key, w_value, w_forget.T, query_gain[None, :],
    ).reshape(rows, width)
    query = proj[:, :nq].astype(BF16).reshape(rows, groups, sharing, HEAD_DIM)
    key_new = proj[:, nq : nq + nk].astype(BF16).reshape(rows, groups, HEAD_DIM)
    value_new = proj[:, nq + nk : nq + 2 * nk].astype(BF16).astype(F32)
    value_new = value_new.reshape(rows, groups, 1, HEAD_DIM)
    forget = proj[:, nq + 2 * nk : nq + 2 * nk + heads].reshape(rows, heads, 1)
    own_score = jnp.sum(
        query.astype(F32) * key_new.astype(F32)[:, :, None, :], axis=-1
    ) * (HEAD_DIM**-0.5)
    own = jnp.concatenate(
        [
            jnp.broadcast_to(value_new, (rows, groups, sharing, HEAD_DIM)).reshape(
                rows, heads, HEAD_DIM
            ),
            jnp.broadcast_to(own_score.reshape(rows, heads, 1), (rows, heads, 32)),
            jnp.broadcast_to(forget, (rows, heads, 32)),
        ],
        axis=-1,
    )
    same = jnp.eye(groups, dtype=jnp.bool_)[None, :, None, :, None]
    spread = jnp.where(same, query[:, :, :, None, :], jnp.zeros((), BF16))
    spread = spread.reshape(rows, heads, groups * HEAD_DIM)
    step = 8
    block = lambda a, b: pl.BlockSpec((step, a, b), lambda i: (i, 0, 0))
    gd = groups * HEAD_DIM
    packed = pl.pallas_call(
        functools.partial(attend_kernel, sharing),
        grid=(rows // step,),
        out_shape=jax.ShapeDtypeStruct((rows, heads, 128), F32),
        in_specs=[block(heads, gd), block(gd, span), block(gd, span), block(heads, span)],
        out_specs=block(heads, 128),
    )(
        spread,
        key_cache.reshape(rows, gd, span),
        value_cache.reshape(rows, gd, span),
        decay_cache,
    )
    ff = w_up.shape[1]
    ffc = ff // n
    return pl.pallas_call(
        functools.partial(rest_kernel, n, t, d),
        out_shape=jax.ShapeDtypeStruct((rows, dl), BF16),
        in_specs=[vmem] * 4 + [anywhere] * 3,
        out_specs=vmem,
        scratch_shapes=[
            pltpu.VMEM(w_out.shape, BF16),
            pltpu.VMEM(w_up.shape, BF16),
            pltpu.VMEM(w_down.shape, BF16),
            pltpu.VMEM((n, rc, heads, 128), F32),
            pltpu.VMEM((rc, nq), BF16),
            pltpu.VMEM((n, rc, nq), BF16),
            pltpu.VMEM((rows, nq), F32),
            pltpu.VMEM((t, rows, dl), BF16),
            pltpu.VMEM((t, rows, dl), BF16),
            pltpu.VMEM((n // 2, rows, ffc), BF16),
            pltpu.VMEM((n // 2, rows, ffc), BF16),
            pltpu.VMEM((n // 2, rows, ffc), BF16),
            pltpu.VMEM((n // 2, rows, ffc), BF16),
            pltpu.VMEM((n // 2, rows, ffc), F32),
            pltpu.VMEM((8, rows), F32),
            pltpu.VMEM((n, 8, rows), F32),
            pltpu.VMEM((n, rows, ffc), BF16),
            dma((3,)), dma((14, n)), dma((4, t)),
        ],
        compiler_params=pltpu.CompilerParams(collective_id=1, has_side_effects=True),
    )(packed, own, tokens, mlp_gain[None, :], w_out, w_up, w_down)


def solution(mesh):
    in_specs = (
        P(None, "kv"),
        P("kv"),
        P("kv", "tp"),
        P("kv", "tp"),
        P("kv", "tp"),
        P("kv", "tp"),
        P(),
        P(None, "tp", None, "kv"),
        P(None, "tp", None, "kv"),
        P(None, "tp", "kv"),
        P("tp", "kv"),
        P("kv"),
        P("kv", "tp"),
        P("tp", "kv"),
    )
    body = functools.partial(shards, mesh.shape["kv"], mesh.shape["tp"])
    return jax.shard_map(
        body, mesh=mesh, in_specs=in_specs, out_specs=P(None, "kv"), check_vma=False
    )
```

profile of v0, /device:TPU:0, one launch (start us, length us, event | category | flops | bytes accessed | tf_op | source)
XLA Modules:
  0.0 90.0 jit_solution(856469708680988134)
XLA Ops:
  0.0 19.8 %shard_map.136 = f32[8,8,896]{2,1,0:T(8,128)} custom-call(bf16[64,512]{1,0:T(8,128)(2,1)} %tok.3, f32[1,512]{1,0:T(1,128)} %bitcast.16, bf16[512,512]{1,0:T(8,128)(2,1)} %wq.1, bf16[512,128]{1,0:T(8,128)(2,1)} %wk.1, bf16[512,128]{1,0:T(8,128)(2,1)} %wv.1, bf16[8,512]{1,0:T(8,128)(2,1)} %bitcast.15, f32[1,64]{1,0:T(1,128)} %bitcast.18), custom_call_target="tpu_custom_call" | custom-call | tf_op jit(solution)/shard_map/pallas_call | solution.py:308
  19.8 1.0 %bitcast_convert_fusion = bf16[64,896]{1,0:T(8,128)(2,1)S(1)} fusion(f32[8,8,896]{2,1,0:T(8,128)} %shard_map.136), kind=kLoop, calls=%fused_computation.7 | loop fusion | flops 57344 | bytes 344064 | tf_op jit(solution)/shard_map/convert.4
  20.8 0.1 broadcast_in_dim.64
  20.9 0.1 reshape.49
  21.0 0.3 multiply_reduce_fusion
  21.3 0.1 copy.18
  21.4 0.1 copy.19
  21.5 0.1 broadcast_in_dim.71
  21.6 0.1 reshape.48
  21.8 0.8 slice.22
  22.5 0.1 broadcast_in_dim.72
  22.7 0.9 %pad_maximum_fusion.own = f32[64,8,128]{2,1,0:T(8,128)} fusion(f32[64,8,32]{2,1,0:T(8,128)S(1)} %broadcast_in_dim.72, f32[64,8,32]{2,1,0:T(8,128)S(1)} %broadcast_in_dim.71, f32[64,8,64]{2,1,0:T(8,128)S(1)} %bitcast.13), kind=kLoop, calls=%fused_computation | loop fusion | flops 131072 | bytes 524288 | tf_op jit(solution)/shard_map/concatenate | solution.py:331
  23.6 0.2 broadcast_in_dim.65
  23.8 0.1 broadcast_in_dim.66
  23.9 0.1 broadcast_in_dim.59
  24.0 0.1 broadcast_in_dim.60
  24.1 0.7 broadcast_select_fusion.q_ref
  24.8 15.8 %shard_map.137.packed = f32[64,8,128]{2,1,0:T(8,128)} custom-call(bf16[64,8,128]{2,1,0:T(8,128)(2,1)} %broadcast_select_fusion.q_ref, bf16[64,128,1024]{2,1,0:T(8,128)(2,1)} %bitcast.10, bf16[64,128,1024]{2,1,0:T(8,128)(2,1)} %bitcast.11, f32[64,8,1024]{2,1,0:T(8,128)} %d_ref.1), custom_call_target="tpu_custom_call" | custom-call | tf_op jit(solution)/shard_map/pallas_call | solution.py:347
  40.6 47.9 %shard_map.138 = bf16[64,512]{1,0:T(8,128)(2,1)} custom-call(f32[64,8,128]{2,1,0:T(8,128)} %shard_map.137.packed, f32[64,8,128]{2,1,0:T(8,128)} %pad_maximum_fusion.own, bf16[64,512]{1,0:T(8,128)(2,1)} %tok.3, f32[1,512]{1,0:T(1,128)} %bitcast.17, bf16[512,512]{1,0:T(8,128)(2,1)} %wo_hbm.1, bf16[512,4096]{1,0:T(8,128)(2,1)} %wu_hbm.1, bf16[4096,512]{1,0:T(8,128)(2,1)} %wd_hbm.1), custom_call_target="tpu_custom_call" | custom-call | tf_op jit(solution)/shard_map/pallas_call | solution.py:361
  88.5 1.5 %copy.21 = bf16[64,512]{1,0:T(8,128)(2,1)} copy(bf16[64,512]{1,0:T(8,128)(2,1)} %shard_map.138) | data formatting | bytes 131072
  (5 shorter events, 0.1 us)
where the time goes:
time: 90.3 us; the launch traced here: 90 us
  Pallas kernels  83.5 us (92%)
  local copies, waits for them, and re-layouts  3.53 us (4%)
  other arithmetic  2.82 us (3%)
    pallas_call x1, Pallas kernels, shards(): pl.pallas_call(functools.partial(rest_kernel, n, t, d), out_shape=jax.Sha...  47.9 us
    pallas_call x1, Pallas kernels, shards(): pl.pallas_call(functools.partial(project_kernel, n, t, d), out_shape=jax....  19.8 us
    pallas_call x1, Pallas kernels, shards(): pl.pallas_call(functools.partial(attend_kernel, sharing), grid=(rows // s...  15.8 us

commit v1 on v0

v1 whole, which is shorter than its diff:
```python
import functools

import jax
import jax.numpy as jnp
from jax import lax
from jax.experimental import pallas as pl
from jax.experimental.pallas import tpu as pltpu
from jax.sharding import PartitionSpec as P

MESH = pl.DeviceIdType.MESH
HEAD_DIM = 64
EPS = 1e-06
DEPTH = 256
F32 = jnp.float32
BF16 = jnp.bfloat16


def greet(n, t):
    kv, tp = lax.axis_index("kv"), lax.axis_index("tp")
    barrier = pltpu.get_barrier_semaphore()
    for i in range(1, n):
        pl.semaphore_signal(
            barrier, inc=1, device_id=(lax.rem(kv + i, n), tp), device_id_type=MESH
        )
    for i in range(1, t):
        pl.semaphore_signal(
            barrier, inc=1, device_id=(kv, lax.rem(tp + i, t)), device_id_type=MESH
        )
    pl.semaphore_wait(barrier, n + t - 2)


def remote(src, dst, send, recv, kv, tp):
    return pltpu.make_async_remote_copy(
        src_ref=src,
        dst_ref=dst,
        send_sem=send,
        recv_sem=recv,
        device_id=(kv, tp),
        device_id_type=MESH,
    )


def split(x):
    hi = x.astype(BF16).astype(F32)
    return hi, (x - hi).astype(BF16).astype(F32)


def layer_kernel(
    n, t, d, sharing,
    mgain, qgain, pgain, tok_hbm, wq_hbm, wk_hbm, wv_hbm, wf_hbm,
    k_hbm, v_hbm, d_hbm, wo_hbm, wu_hbm, wd_hbm, out,
    tok, wq, wk, wv, wf, kbuf, vbuf, dbuf, wo, wu, wd,
    partq, partx, gotq, gotx, qs, qall, own, msg, gotm, heads_s,
    att, allatt, full, tpa, tpb, upsend, upgot, upsend2, upgot2, keep, sqs, sqgot, hid,
    wsem, ksem, vsem, dsem, sem, tsem,
):
    kv, tp = lax.axis_index("kv"), lax.axis_index("tp")
    rows, dl = tok.shape
    rc = rows // n
    nq, nk, heads = wq.shape[1], wk.shape[1], wf.shape[0]
    gd = (heads // sharing) * HEAD_DIM
    lines = rc * heads
    pack = DEPTH // gd
    tile = pack * heads

    def local(src, dst, s):
        return pltpu.make_async_copy(src, dst, s)

    def block_of(i):
        return lax.rem(kv + i, n)

    first = [
        local(a, b, wsem.at[j])
        for j, (a, b) in enumerate(
            ((tok_hbm, tok), (wq_hbm, wq), (wk_hbm, wk), (wv_hbm, wv), (wf_hbm, wf))
        )
    ]
    for c in first:
        c.start()

    def cache_loads(i):
        b = block_of(i)
        at = pl.ds(pl.multiple_of(b * rc * gd, rc * gd), rc * gd)
        lt = pl.ds(pl.multiple_of(b * lines, lines), lines)
        return (
            local(k_hbm.at[at], kbuf.at[at], ksem.at[i]),
            local(d_hbm.at[lt], dbuf.at[lt], dsem.at[i]),
            local(v_hbm.at[at], vbuf.at[at], vsem.at[i]),
        )

    for i in list(range(1, n)) + [0]:
        for c in cache_loads(i):
            c.start()
    late = [
        local(a, b, wsem.at[5 + j])
        for j, (a, b) in enumerate(((wo_hbm, wo), (wu_hbm, wu), (wd_hbm, wd)))
    ]
    for c in late:
        c.start()
    greet(n, t)
    started = []

    def send(kind, i, src, dst, peer=None):
        if peer is None:
            peer = lax.rem(kv + i, n)
        c = remote(src(peer), dst, sem.at[2 * kind, i], sem.at[2 * kind + 1, i], peer, tp)
        c.start()
        started.append(c)
        return c

    for c in first:
        c.wait()
    stream = tok[...].astype(F32)
    squares = jnp.sum(stream * stream, axis=1, keepdims=True)
    normed = (stream * mgain[...]).astype(BF16)
    q = jnp.dot(normed, wq[...], preferred_element_type=F32)
    f = lax.dot_general(
        normed, wf[...], (((1,), (1,)), ((), ())), preferred_element_type=F32
    )
    for p in range(n):
        cut = slice(p * rc, (p + 1) * rc)
        partq[p, :, 0:nq] = q[cut]
        partq[p, :, nq : nq + 128] = jnp.broadcast_to(squares[cut], (rc, 128))
        partq[p, :, nq : nq + heads] = f[cut]
    qcopies = [send(0, i, lambda p: partq.at[p], gotq.at[i]) for i in range(1, n)]
    k = jnp.dot(normed, wk[...], preferred_element_type=F32)
    v = jnp.dot(normed, wv[...], preferred_element_type=F32)
    for p in range(n):
        cut = slice(p * rc, (p + 1) * rc)
        partx[p, :, 0:nk] = k[cut]
        partx[p, :, nk : 2 * nk] = v[cut]
    xcopies = [send(1, i, lambda p: partx.at[p], gotx.at[i]) for i in range(1, n)]

    total = partq[kv]
    for c in qcopies:
        c.wait_recv()
    for i in range(1, n):
        total = total + gotq[i]
    scale = lax.rsqrt(total[:, nq + 127 : nq + 128] / d + EPS)
    raw = total[:, 0:nq] * scale
    gate = total[:, nq : nq + heads] * scale
    forget = jnp.minimum(gate, 0.0) - jnp.log1p(jnp.exp(-jnp.abs(gate)))
    queries = []
    for h in range(heads):
        part = raw[:, h * HEAD_DIM : (h + 1) * HEAD_DIM]
        mean = jnp.sum(part * part, axis=1, keepdims=True) / HEAD_DIM
        part = (part * lax.rsqrt(mean + EPS) * qgain[...]).astype(BF16).astype(F32)
        queries.append(part)
        g = h // sharing
        pieces = [part if j == g else jnp.zeros_like(part) for j in range(heads // sharing)]
        wide = jnp.concatenate(pieces, axis=1) if len(pieces) > 1 else part
        qs[pl.ds(h, rc, stride=heads), :] = wide
    qall[kv] = qs[...].astype(BF16)
    gathers = [send(2, i, lambda p: qall.at[kv], qall.at[kv]) for i in range(1, n)]
    extra = partx[kv]
    for c in xcopies:
        c.wait_recv()
    for i in range(1, n):
        extra = extra + gotx[i]
    extra = (extra * scale).astype(BF16).astype(F32)
    for h in range(heads):
        g = h // sharing
        key = extra[:, g * HEAD_DIM : (g + 1) * HEAD_DIM]
        value = extra[:, nk + g * HEAD_DIM : nk + (g + 1) * HEAD_DIM]
        score = jnp.sum(queries[h] * key, axis=1, keepdims=True) * (HEAD_DIM**-0.5)
        own[pl.ds(h, rc, stride=heads), :] = jnp.concatenate(
            [
                value,
                jnp.broadcast_to(score, (rc, 32)),
                jnp.broadcast_to(forget[:, h : h + 1], (rc, 32)),
            ],
            axis=1,
        )

    line = lax.broadcasted_iota(jnp.int32, (tile, gd), 0) // heads
    slot = lax.broadcasted_iota(jnp.int32, (tile, HEAD_DIM), 0) // sharing
    lane = lax.broadcasted_iota(jnp.int32, (tile, HEAD_DIM), 1) // 16

    def attend(b):
        steps = lines // tile
        scores, sums, peaks, outs = [], [], [], []
        for s in range(steps):
            qt = qall[b, s * tile : (s + 1) * tile, :]
            left = jnp.concatenate(
                [jnp.where(line == j, qt, jnp.zeros_like(qt)) for j in range(pack)], axis=1
            )
            at = pl.ds(pl.multiple_of(b * rc * gd + s * DEPTH, DEPTH), DEPTH)
            lt = pl.ds(pl.multiple_of(b * lines + s * tile, tile), tile)
            scores.append(
                jnp.dot(left, kbuf[at, :], preferred_element_type=F32) * (HEAD_DIM**-0.5)
                + dbuf[lt, :]
            )
        weights = []
        for s in range(steps):
            hi, lo = split(jnp.max(scores[s], axis=1, keepdims=True))
            w = jnp.exp(scores[s] - (hi + lo))
            peaks.append((hi, lo))
            sums.append(split(jnp.sum(w, axis=1, keepdims=True)))
            weights.append(w.astype(BF16))
        for s in range(steps):
            at = pl.ds(pl.multiple_of(b * rc * gd + s * DEPTH, DEPTH), DEPTH)
            o = lax.dot_general(
                weights[s], vbuf[at, :], (((1,), (1,)), ((), ())), preferred_element_type=F32
            )
            picked = o[:, 0:HEAD_DIM]
            for g in range(1, DEPTH // HEAD_DIM):
                picked = jnp.where(slot == g, o[:, g * HEAD_DIM : (g + 1) * HEAD_DIM], picked)
            stats = jnp.where(
                lane == 0,
                peaks[s][0],
                jnp.where(lane == 1, peaks[s][1], jnp.where(lane == 2, sums[s][0], sums[s][1])),
            )
            msg[b, s * tile : (s + 1) * tile, :] = jnp.concatenate(
                [picked, stats], axis=1
            ).astype(BF16)

    def message(i):
        b = block_of(i)
        return remote(msg.at[b], gotm.at[i], sem.at[6, i], sem.at[7, i], b, tp)

    def step(i, carry):
        b = block_of(i)
        remote(
            qall.at[b], qall.at[b], sem.at[4, n - i], sem.at[5, n - i], b, tp
        ).wait_recv()
        for c in cache_loads(i):
            c.wait()
        attend(b)
        message(i).start()
        return carry

    lax.fori_loop(1, n, step, 0)
    for c in cache_loads(0):
        c.wait()
    attend(kv)

    extra = own[...]
    own_score = extra[:, 64:65]
    forget = extra[:, 96:97]
    for i in range(1, n):
        message(i).wait_recv()
    blocks = [msg[kv].astype(F32)] + [gotm[i].astype(F32) for i in range(1, n)]
    peaks = [b[:, 64:65] + b[:, 80:81] + forget for b in blocks]
    peak = own_score
    for p in peaks:
        peak = jnp.maximum(peak, p)
    own_weight = jnp.exp(own_score - peak)
    mass = own_weight
    summed = own_weight.astype(BF16).astype(F32) * extra[:, 0:64]
    for b, p in zip(blocks, peaks):
        w = jnp.exp(p - peak)
        mass = mass + w * (b[:, 96:97] + b[:, 112:113])
        summed = summed + w * b[:, 0:64]
    heads_s[...] = summed / mass
    for h in range(0, heads, 2):
        att[:, h * HEAD_DIM : (h + 2) * HEAD_DIM] = jnp.concatenate(
            [
                heads_s[pl.ds(h, rc, stride=heads), :],
                heads_s[pl.ds(h + 1, rc, stride=heads), :],
            ],
            axis=1,
        ).astype(BF16)

    def tp_sum(kind, buf, value):
        buf[tp] = value.astype(BF16)
        copies = []
        for i in range(1, t):
            c = remote(
                buf.at[tp], buf.at[tp], tsem.at[2 * kind, i], tsem.at[2 * kind + 1, i],
                kv, lax.rem(tp + i, t),
            )
            c.start()
            copies.append(c)
            started.append(c)
        for c in copies:
            c.wait_recv()
        total = buf[0].astype(F32)
        for j in range(1, t):
            total = total + buf[j].astype(F32)
        return total.astype(BF16).astype(F32)

    ffc = wu.shape[1] // n
    copies = [send(4, i, lambda p: att, allatt.at[kv]) for i in range(1, n)]
    allatt[kv] = att[...]
    late[0].wait()
    for c in copies:
        c.wait_recv()
    for p in range(n):
        full[p * rc : (p + 1) * rc, :] = allatt[p].astype(F32)
    attn = jnp.dot(full[...].astype(BF16), wo[...], preferred_element_type=F32)
    attn = tp_sum(0, tpa, attn)
    residual = (tok[...].astype(F32) + attn).astype(BF16).astype(F32)
    normed = (residual * pgain[...]).astype(BF16)
    late[1].wait()
    half = n // 2
    side = lax.rem(kv, 2)
    place = kv // 2
    partner = kv + 1 - 2 * side
    order = list(range(1, half)) + [0]

    def term(dest):
        cols = pl.ds(pl.multiple_of(dest * ffc, ffc), ffc)
        return jnp.dot(normed, wu[:, cols], preferred_element_type=F32)

    firsts = {}
    for j in order:
        upsend[j] = term(2 * lax.rem(place + j, half) + 1 - side).astype(BF16)
        firsts[j] = send(5, j, lambda p: upsend.at[j], upgot.at[j], partner)
    for j in order:
        keep[j] = term(2 * lax.rem(place + j, half) + side)
    sqs[...] = lax.dot_general(
        jnp.ones((8, residual.shape[1]), F32),
        residual * residual,
        (((1,), (1,)), ((), ())),
        preferred_element_type=F32,
        precision=lax.Precision.HIGHEST,
    )
    sq_copies = [send(6, i, lambda p: sqs, sqgot.at[i]) for i in range(1, n)]
    seconds = {}
    for j in order:
        firsts[j].wait_recv()
        part = keep[j] + upgot[j].astype(F32)
        if j:
            upsend2[j] = part.astype(BF16)
            seconds[j] = send(
                7, j, lambda p: upsend2.at[j], upgot2.at[j], 2 * lax.rem(place + j, half) + side
            )
    total = sqs[...]
    for i in range(1, n):
        sq_copies[i - 1].wait_recv()
        total = total + sqgot[i]
    r = lax.broadcasted_iota(jnp.int32, (rows, rows), 0)
    c_ = lax.broadcasted_iota(jnp.int32, (rows, rows), 1)
    wide = jnp.broadcast_to(total[0:1, :], (rows, rows))
    column = jnp.sum(jnp.where(r == c_, wide, 0.0), axis=1, keepdims=True)
    scale = lax.rsqrt(column / d + EPS)
    for j in range(1, half):
        seconds[j].wait_recv()
        part = part + upgot2[j].astype(F32)
    hidden = jnp.square(jnp.maximum(part * scale, 0.0)).astype(BF16)
    hid[kv] = hidden
    across = {0: send(9, 0, lambda p: hid.at[kv], hid.at[kv], partner)}
    along = {}
    for j in range(1, half):
        along[j] = send(
            8, j, lambda p: hid.at[kv], hid.at[kv], 2 * lax.rem(place + j, half) + side
        )
    late[2].wait()

    def lower(src):
        there = pl.ds(pl.multiple_of(src * ffc, ffc), ffc)
        return jnp.dot(hid[src], wd[there, :], preferred_element_type=F32)

    down = lower(kv)
    for j in range(1, half):
        src = 2 * lax.rem(place + half - j, half) + side
        along[j].wait_recv()
        across[j] = send(9, j, lambda p: hid.at[src], hid.at[src], partner)
        down = down + lower(src)
    for j in range(half):
        across[j].wait_recv()
        down = down + lower(2 * lax.rem(place + half - j, half) + 1 - side)
    mlp = tp_sum(1, tpb, down)
    out[...] = (residual + mlp).astype(BF16)
    for i in range(1, n):
        message(i).wait_send()
    for c in started:
        c.wait_send()


def shards(
    n, t, tokens, mix_gain, w_query, w_key, w_value, w_forget, query_gain,
    key_cache, value_cache, decay_cache, w_out, mlp_gain, w_up, w_down,
):
    rows, dl = tokens.shape
    d = dl * n
    rc = rows // n
    heads = w_forget.shape[1]
    groups = key_cache.shape[1]
    sharing = heads // groups
    nq, nk = w_query.shape[1], w_key.shape[1]
    span = key_cache.shape[3]
    gd = groups * HEAD_DIM
    ffc = w_up.shape[1] // n
    half = n // 2
    vmem = pl.BlockSpec(memory_space=pltpu.VMEM)
    anywhere = pl.BlockSpec(memory_space=pl.ANY)
    dma = pltpu.SemaphoreType.DMA
    return pl.pallas_call(
        functools.partial(layer_kernel, n, t, d, sharing),
        out_shape=jax.ShapeDtypeStruct((rows, dl), BF16),
        in_specs=[vmem] * 3 + [anywhere] * 11,
        out_specs=vmem,
        scratch_shapes=[
            pltpu.VMEM(tokens.shape, BF16),
            pltpu.VMEM(w_query.shape, BF16),
            pltpu.VMEM(w_key.shape, BF16),
            pltpu.VMEM(w_value.shape, BF16),
            pltpu.VMEM((heads, dl), BF16),
            pltpu.VMEM((rows * gd, span), BF16),
            pltpu.VMEM((rows * gd, span), BF16),
            pltpu.VMEM((rows * heads, span), F32),
            pltpu.VMEM(w_out.shape, BF16),
            pltpu.VMEM(w_up.shape, BF16),
            pltpu.VMEM(w_down.shape, BF16),
            pltpu.VMEM((n, rc, nq + 128), F32),
            pltpu.VMEM((n, rc, 2 * nk), F32),
            pltpu.VMEM((n, rc, nq + 128), F32),
            pltpu.VMEM((n, rc, 2 * nk), F32),
            pltpu.VMEM((rc * heads, gd), F32),
            pltpu.VMEM((n, rc * heads, gd), BF16),
            pltpu.VMEM((rc * heads, 128), F32),
            pltpu.VMEM((n, rc * heads, 128), BF16),
            pltpu.VMEM((n, rc * heads, 128), BF16),
            pltpu.VMEM((rc * heads, HEAD_DIM), F32),
            pltpu.VMEM((rc, nq), BF16),
            pltpu.VMEM((n, rc, nq), BF16),
            pltpu.VMEM((rows, nq), F32),
            pltpu.VMEM((t, rows, dl), BF16),
            pltpu.VMEM((t, rows, dl), BF16),
            pltpu.VMEM((half, rows, ffc), BF16),
            pltpu.VMEM((half, rows, ffc), BF16),
            pltpu.VMEM((half, rows, ffc), BF16),
            pltpu.VMEM((half, rows, ffc), BF16),
            pltpu.VMEM((half, rows, ffc), F32),
            pltpu.VMEM((8, rows), F32),
            pltpu.VMEM((n, 8, rows), F32),
            pltpu.VMEM((n, rows, ffc), BF16),
            dma((8,)), dma((n,)), dma((n,)), dma((n,)), dma((20, n)), dma((4, t)),
        ],
        compiler_params=pltpu.CompilerParams(
            collective_id=0, has_side_effects=True, vmem_limit_bytes=60 * 2**20
        ),
    )(
        mix_gain[None, :], query_gain[None, :], mlp_gain[None, :],
        tokens, w_query, w_key, w_value, w_forget.T,
        key_cache.reshape(rows * gd, span),
        value_cache.reshape(rows * gd, span),
        decay_cache.reshape(rows * heads, span),
        w_out, w_up, w_down,
    )


def solution(mesh):
    in_specs = (
        P(None, "kv"),
        P("kv"),
        P("kv", "tp"),
        P("kv", "tp"),
        P("kv", "tp"),
        P("kv", "tp"),
        P(),
        P(None, "tp", None, "kv"),
        P(None, "tp", None, "kv"),
        P(None, "tp", "kv"),
        P("tp", "kv"),
        P("kv"),
        P("kv", "tp"),
        P("tp", "kv"),
    )
    body = functools.partial(shards, mesh.shape["kv"], mesh.shape["tp"])
    return jax.shard_map(
        body, mesh=mesh, in_specs=in_specs, out_specs=P(None, "kv"), check_vma=False
    )
```

time: 90.3 us -> 68.4 us (0.76)
  Pallas kernels: 83.5 us -> 66 us
  other arithmetic: 2.82 us -> 0 us
  local copies, waits for them, and re-layouts: 3.53 us -> 1.47 us
    pallas_call x3 -> x1, Pallas kernels: 83.5 us -> 66 us  [shards(): pl.pallas_call(functools.partial(layer_kernel, n, t, d, sharing), out_sha...]
    broadcast_in_dim x9 -> x0, local copies, waits for them, and re-layouts: 1.02 us -> none  [the longest x5 0.62 us: shards(): spread = jnp.where(same, query[:, :, :, None, :], jnp.zeros((), BF16))]
    another operation x1 -> x0, other arithmetic: 0.95 us -> none
    concatenate x1 -> x0, other arithmetic: 0.91 us -> none  [shards(): jnp.concatenate([jnp.broadcast_to(value_new, (rows, groups, sharing, HEAD...]
where the time goes in v1:
time: 68.4 us; the launch traced here: 67.4 us
  Pallas kernels  66 us (96%)
  local copies, waits for them, and re-layouts  1.47 us (2%)
    pallas_call x1, Pallas kernels, shards(): pl.pallas_call(functools.partial(layer_kernel, n, t, d, sharing), out_sha...  66 us
    unnamed x1, local copies, waits for them, and re-layouts  1.47 us

profile of v1, /device:TPU:0, one launch (start us, length us, event | category | flops | bytes accessed | tf_op | source)
XLA Modules:
  0.0 67.4 jit_solution(12259672922494584624)
XLA Ops:
  0.0 66.0 %shard_map.136 = bf16[64,512]{1,0:T(8,128)(2,1)} custom-call(f32[1,512]{1,0:T(1,128)} %bitcast.11, f32[1,64]{1,0:T(1,128)} %bitcast.13, f32[1,512]{1,0:T(1,128)} %bitcast.12, bf16[64,512]{1,0:T(8,128)(2,1)} %tok_hbm.1, bf16[512,512]{1,0:T(8,128)(2,1)} %wq_hbm.1, bf16[512,128]{1,0:T(8,128)(2,1)} %wk_hbm.1, bf16[512,128]{1,0:T(8,128)(2,1)} %wv_hbm.1, ...), custom_call_target="tpu_custom_call" | custom-call | tf_op jit(solution)/shard_map/pallas_call | solution.py:389
  66.0 1.5 %copy.16 = bf16[64,512]{1,0:T(8,128)(2,1)} copy(bf16[64,512]{1,0:T(8,128)(2,1)} %shard_map.136) | data formatting | bytes 131072

commit v2 on v1

v2 whole, which is shorter than its diff:
```python
import functools

import jax
import jax.numpy as jnp
from jax import lax
from jax.experimental import pallas as pl
from jax.experimental.pallas import tpu as pltpu
from jax.sharding import PartitionSpec as P

MESH = pl.DeviceIdType.MESH
HEAD_DIM = 64
EPS = 1e-06
DEPTH = 256
F32 = jnp.float32
BF16 = jnp.bfloat16


def greet(n, t):
    kv, tp = lax.axis_index("kv"), lax.axis_index("tp")
    barrier = pltpu.get_barrier_semaphore()
    for i in range(1, n):
        pl.semaphore_signal(
            barrier, inc=1, device_id=(lax.rem(kv + i, n), tp), device_id_type=MESH
        )
    for i in range(1, t):
        pl.semaphore_signal(
            barrier, inc=1, device_id=(kv, lax.rem(tp + i, t)), device_id_type=MESH
        )
    pl.semaphore_wait(barrier, n + t - 2)


def remote(src, dst, send, recv, kv, tp):
    return pltpu.make_async_remote_copy(
        src_ref=src,
        dst_ref=dst,
        send_sem=send,
        recv_sem=recv,
        device_id=(kv, tp),
        device_id_type=MESH,
    )


def semaphores(n, parts):
    half = n // 2
    sizes = dict(
        first=5, late=3, cache=3 * parts, q=2, x=2, g=2, m=1 + parts, a=1 + parts,
        t0=1 + parts, t1=1 + parts, y=1 + parts * half, s=1 + parts, z=1 + parts,
        along=1 + parts * half, across=1 + parts * half,
    )
    at, total = {}, 0
    for name, size in sizes.items():
        at[name] = total
        total += size
    return at, total


def split(x):
    hi = x.astype(BF16).astype(F32)
    return hi, (x - hi).astype(BF16).astype(F32)


def layer_kernel(
    n, t, d, sharing, parts,
    mgain, qgain, pgain, tok_hbm, wq_hbm, wk_hbm, wv_hbm, wf_hbm,
    k_hbm, v_hbm, d_hbm, wo_hbm, wu_hbm, wd_hbm, out,
    tok, wq, wk, wv, wf, kbuf, vbuf, dbuf, wo, wu, wd,
    partq, partx, gotq, gotx, qs, qall, own, msg, gotm, heads_s,
    att, allatt, full, tpa, tpb, upsend, upgot, upsend2, upgot2, keep, sqs, sqgot, hid,
    sem,
):
    kv, tp = lax.axis_index("kv"), lax.axis_index("tp")
    rows, dl = tok.shape
    rc = rows // n
    rh = rows // parts
    rb = rh // n
    nq, nk, heads = wq.shape[1], wk.shape[1], wf.shape[0]
    groups = heads // sharing
    gd = groups * HEAD_DIM
    lines = rb * heads
    pack = DEPTH // gd
    tile = pack * heads
    ffc = wu.shape[1] // n

    at_sem, _ = semaphores(n, parts)

    def flag(name, i=0):
        return sem.at[at_sem[name] + i]

    def local(src, dst, s):
        return pltpu.make_async_copy(src, dst, s)

    def drain(ref, s):
        pltpu.make_async_copy(ref, ref, s).wait()

    def block_of(i):
        return lax.rem(kv + i, n)

    first = [
        local(a, b, flag("first", j))
        for j, (a, b) in enumerate(
            ((tok_hbm, tok), (wq_hbm, wq), (wk_hbm, wk), (wv_hbm, wv), (wf_hbm, wf))
        )
    ]
    for c in first:
        c.start()

    def cache_loads(h):
        at = pl.ds(h * rh * gd, rh * gd)
        lt = pl.ds(h * rh * heads, rh * heads)
        return (
            local(k_hbm.at[at], kbuf.at[at], flag("cache", 3 * h)),
            local(d_hbm.at[lt], dbuf.at[lt], flag("cache", 3 * h + 1)),
            local(v_hbm.at[at], vbuf.at[at], flag("cache", 3 * h + 2)),
        )

    for h in range(parts):
        for c in cache_loads(h):
            c.start()
    late = [
        local(a, b, flag("late", j))
        for j, (a, b) in enumerate(((wo_hbm, wo), (wu_hbm, wu), (wd_hbm, wd)))
    ]
    for c in late:
        c.start()
    greet(n, t)

    def send(name, src, dst, peer, slot=0):
        remote(src, dst, flag(name), flag(name, 1 + slot), peer, tp).start()

    def to_all(name, src, dst, slot=0):
        for i in range(1, n):
            peer = lax.rem(kv + i, n)
            send(name, src(peer), dst(i), peer, slot)

    for c in first:
        c.wait()
    stream = tok[...].astype(F32)
    squares = jnp.sum(stream * stream, axis=1, keepdims=True)
    normed = (stream * mgain[...]).astype(BF16)
    q = jnp.dot(normed, wq[...], preferred_element_type=F32)
    f = lax.dot_general(
        normed, wf[...], (((1,), (1,)), ((), ())), preferred_element_type=F32
    )
    pieces = [
        (p, slice(h * rb, (h + 1) * rb), slice(h * rh + p * rb, h * rh + (p + 1) * rb))
        for p in range(n)
        for h in range(parts)
    ]
    for p, to, cut in pieces:
        partq[p, to, 0:nq] = q[cut]
        partq[p, to, nq : nq + 128] = jnp.broadcast_to(squares[cut], (rb, 128))
        partq[p, to, nq : nq + heads] = f[cut]
    to_all("q", lambda p: partq.at[p], lambda i: gotq.at[i])
    k = jnp.dot(normed, wk[...], preferred_element_type=F32)
    v = jnp.dot(normed, wv[...], preferred_element_type=F32)
    for p, to, cut in pieces:
        partx[p, to, 0:nk] = k[cut]
        partx[p, to, nk : 2 * nk] = v[cut]
    to_all("x", lambda p: partx.at[p], lambda i: gotx.at[i])

    total = partq[kv]
    others = pl.ds(1, n - 1)
    drain(gotq.at[others], flag("q", 1))
    for i in range(1, n):
        total = total + gotq[i]
    scale = lax.rsqrt(total[:, nq + 127 : nq + 128] / d + EPS)
    raw = total[:, 0:nq] * scale
    gate = total[:, nq : nq + heads] * scale
    forget = jnp.minimum(gate, 0.0) - jnp.log1p(jnp.exp(-jnp.abs(gate)))
    queries = []
    for h in range(heads):
        part = raw[:, h * HEAD_DIM : (h + 1) * HEAD_DIM]
        mean = jnp.sum(part * part, axis=1, keepdims=True) / HEAD_DIM
        part = (part * lax.rsqrt(mean + EPS) * qgain[...]).astype(BF16).astype(F32)
        queries.append(part)
    for j in range(sharing):
        side_by_side = [queries[g * sharing + j] for g in range(groups)]
        qs[pl.ds(j, rc, stride=sharing), :] = (
            jnp.concatenate(side_by_side, axis=1) if groups > 1 else side_by_side[0]
        )
    for h in range(parts):
        qall[kv, h] = qs[h * rb * sharing : (h + 1) * rb * sharing, :].astype(BF16)
    to_all("g", lambda p: qall.at[kv], lambda i: qall.at[kv])
    extra = partx[kv]
    drain(gotx.at[others], flag("x", 1))
    for i in range(1, n):
        extra = extra + gotx[i]
    extra = (extra * scale).astype(BF16).astype(F32)
    for h in range(heads):
        g = h // sharing
        key = extra[:, g * HEAD_DIM : (g + 1) * HEAD_DIM]
        value = extra[:, nk + g * HEAD_DIM : nk + (g + 1) * HEAD_DIM]
        score = jnp.sum(queries[h] * key, axis=1, keepdims=True) * (HEAD_DIM**-0.5)
        own[pl.ds(h, rc, stride=heads), :] = jnp.concatenate(
            [
                value,
                jnp.broadcast_to(score, (rc, 32)),
                jnp.broadcast_to(forget[:, h : h + 1], (rc, 32)),
            ],
            axis=1,
        )

    group_row = lax.broadcasted_iota(jnp.int32, (heads, gd), 0) // sharing
    group_lane = lax.broadcasted_iota(jnp.int32, (heads, gd), 1) // HEAD_DIM
    slot = lax.broadcasted_iota(jnp.int32, (tile, HEAD_DIM), 0) // sharing
    lane = lax.broadcasted_iota(jnp.int32, (tile, HEAD_DIM), 1) // 16

    def attend(h, bs):
        todo = [(b, s) for b in bs for s in range(lines // tile)]
        scores, sums, peaks = [], [], []
        for b, s in todo:
            qt = qall[b, h].astype(F32)
            strips = []
            for j in range(pack):
                at = (s * pack + j) * sharing
                one = jnp.concatenate([qt[at : at + sharing]] * groups, axis=0)
                one = jnp.where(group_row == group_lane, one, 0.0)
                zero = jnp.zeros_like(one)
                strips.append(
                    jnp.concatenate([one if m == j else zero for m in range(pack)], axis=1)
                )
            left = jnp.concatenate(strips, axis=0).astype(BF16)
            row = h * rh + b * rb + s * pack
            at = pl.ds(pl.multiple_of(row * gd, DEPTH), DEPTH)
            lt = pl.ds(pl.multiple_of(row * heads, tile), tile)
            scores.append(
                jnp.dot(left, kbuf[at, :], preferred_element_type=F32) * (HEAD_DIM**-0.5)
                + dbuf[lt, :]
            )
        weights = []
        for sc in scores:
            hi, lo = split(jnp.max(sc, axis=1, keepdims=True))
            w = jnp.exp(sc - (hi + lo))
            peaks.append((hi, lo))
            sums.append(split(jnp.sum(w, axis=1, keepdims=True)))
            weights.append(w.astype(BF16))
        for (b, s), w, top, mass in zip(todo, weights, peaks, sums):
            row = h * rh + b * rb + s * pack
            at = pl.ds(pl.multiple_of(row * gd, DEPTH), DEPTH)
            o = lax.dot_general(
                w, vbuf[at, :], (((1,), (1,)), ((), ())), preferred_element_type=F32
            )
            picked = o[:, 0:HEAD_DIM]
            for g in range(1, DEPTH // HEAD_DIM):
                picked = jnp.where(slot == g, o[:, g * HEAD_DIM : (g + 1) * HEAD_DIM], picked)
            stats = jnp.where(
                lane == 0,
                top[0],
                jnp.where(lane == 1, top[1], jnp.where(lane == 2, mass[0], mass[1])),
            )
            msg[h, b, s * tile : (s + 1) * tile, :] = jnp.concatenate(
                [picked, stats], axis=1
            ).astype(BF16)

    twin = n // 2

    def step(u, h):
        i0 = 1 + 2 * u
        i1 = lax.rem(i0 + 1, n)
        attend(h, [block_of(i0), block_of(i1)])

        def message(i):
            b = block_of(i)
            send("m", msg.at[h, b], gotm.at[h, i], b, h)

        message(i0)

        @pl.when(i1 != 0)
        def _():
            message(i1)

        return h

    def attend_half(h, start, stop):
        lax.fori_loop(start, stop, lambda u, carry: step(u, h) * 0, 0)

    def combine(h):
        extra = own[h * lines : (h + 1) * lines, :]
        own_score = extra[:, 64:65]
        forget = extra[:, 96:97]
        drain(gotm.at[h, others], flag("m", 1 + h))
        blocks = [msg[h, kv].astype(F32)] + [gotm[h, i].astype(F32) for i in range(1, n)]
        peaks = [b[:, 64:65] + b[:, 80:81] + forget for b in blocks]
        peak = own_score
        for p in peaks:
            peak = jnp.maximum(peak, p)
        own_weight = jnp.exp(own_score - peak)
        mass = own_weight
        summed = own_weight.astype(BF16).astype(F32) * extra[:, 0:64]
        for b, p in zip(blocks, peaks):
            w = jnp.exp(p - peak)
            mass = mass + w * (b[:, 96:97] + b[:, 112:113])
            summed = summed + w * b[:, 0:64]
        heads_s[h] = summed / mass
        for j in range(0, heads, 2):
            pair = [heads_s[h, pl.ds(j + m, rb, stride=heads), :] for m in range(2)]
            att[h, :, j * HEAD_DIM : (j + 2) * HEAD_DIM] = jnp.concatenate(
                pair, axis=1
            ).astype(BF16)
        allatt[h, kv] = att[h]
        to_all("a", lambda p: att.at[h], lambda i: allatt.at[h, kv], h)

    def tp_send(name, h, buf, value):
        buf[h, tp] = value.astype(BF16)
        for i in range(1, t):
            remote(
                buf.at[h, tp], buf.at[h, tp], flag(name), flag(name, 1 + h),
                kv, lax.rem(tp + i, t),
            ).start()

    def tp_total(name, h, buf):
        drain(buf.at[h, pl.ds(1, t - 1)], flag(name, 1 + h))
        total = buf[h, 0].astype(F32)
        for j in range(1, t):
            total = total + buf[h, j].astype(F32)
        return total.astype(BF16).astype(F32)

    def project_out(h):
        drain(allatt.at[h, others], flag("a", 1 + h))
        for p in range(n):
            full[h, p * rb : (p + 1) * rb, :] = allatt[h, p].astype(F32)
        attn = jnp.dot(full[h].astype(BF16), wo[...], preferred_element_type=F32)
        tp_send("t0", h, tpa, attn)

    half = n // 2
    side = lax.rem(kv, 2)
    place = kv // 2
    partner = kv + 1 - 2 * side
    order = list(range(1, half)) + [0]

    def up_start(h):
        attn = tp_total("t0", h, tpa)
        residual = (tok[h * rh : (h + 1) * rh, :].astype(F32) + attn).astype(BF16).astype(F32)
        normed = (residual * pgain[...]).astype(BF16)

        def term(dest):
            cols = pl.ds(pl.multiple_of(dest * ffc, ffc), ffc)
            return jnp.dot(normed, wu[:, cols], preferred_element_type=F32)

        for j in order:
            upsend[h, j] = term(2 * lax.rem(place + j, half) + 1 - side).astype(BF16)
            send("y", upsend.at[h, j], upgot.at[h, j], partner, h * half + j)
        for j in order:
            keep[h, j] = term(2 * lax.rem(place + j, half) + side)
        sqs[h] = lax.dot_general(
            jnp.ones((8, dl), F32),
            residual * residual,
            (((1,), (1,)), ((), ())),
            preferred_element_type=F32,
            precision=lax.Precision.HIGHEST,
        )
        to_all("s", lambda p: sqs.at[h], lambda i: sqgot.at[h, i], h)
        return residual

    def up_middle(h):
        for j in order:
            drain(upgot.at[h, j], flag("y", 1 + h * half + j))
            part = keep[h, j] + upgot[h, j].astype(F32)
            if j:
                upsend2[h, j] = part.astype(BF16)
                send(
                    "z", upsend2.at[h, j], upgot2.at[h, j],
                    2 * lax.rem(place + j, half) + side, h,
                )
        return part

    def up_finish(h, part):
        drain(sqgot.at[h, others], flag("s", 1 + h))
        total = sqs[h]
        for i in range(1, n):
            total = total + sqgot[h, i]
        r = lax.broadcasted_iota(jnp.int32, (rh, rh), 0)
        c_ = lax.broadcasted_iota(jnp.int32, (rh, rh), 1)
        wide = jnp.broadcast_to(total[0:1, :], (rh, rh))
        column = jnp.sum(jnp.where(r == c_, wide, 0.0), axis=1, keepdims=True)
        scale = lax.rsqrt(column / d + EPS)
        drain(upgot2.at[h, pl.ds(1, half - 1)], flag("z", 1 + h))
        for j in range(1, half):
            part = part + upgot2[h, j].astype(F32)
        hid[h, kv] = jnp.square(jnp.maximum(part * scale, 0.0)).astype(BF16)
        mine = hid.at[h, kv]
        send("across", mine, mine, partner, h * half)
        for j in range(1, half):
            send("along", mine, mine, 2 * lax.rem(place + j, half) + side, h * half + j)

    def lower(h, src):
        there = pl.ds(pl.multiple_of(src * ffc, ffc), ffc)
        return jnp.dot(hid[h, src], wd[there, :], preferred_element_type=F32)

    def down_start(h):
        down = lower(h, kv)
        for j in range(1, half):
            src = 2 * lax.rem(place + half - j, half) + side
            block = hid.at[h, src]
            drain(block, flag("along", 1 + h * half + j))
            send("across", block, block, partner, h * half + j)
            down = down + lower(h, src)
        return down

    def down_finish(h, down):
        for j in range(half):
            src = 2 * lax.rem(place + half - j, half) + 1 - side
            drain(hid.at[h, src], flag("across", 1 + h * half + j))
            down = down + lower(h, src)
        tp_send("t1", h, tpb, down)

    each = range(parts)
    last = parts - 1
    drain(qall.at[others], flag("g", 1))
    for h in each:
        for c in cache_loads(h):
            c.wait()
        if h < last or parts == 1:
            attend_half(h, 0, twin)
        else:
            attend_half(h, 0, twin // 2)
            for e in range(last):
                combine(e)
            attend_half(h, twin // 2, twin)
    combine(last)
    late[0].wait()
    for h in each:
        project_out(h)
    late[1].wait()
    residuals = {h: up_start(h) for h in each}
    mids = {h: up_middle(h) for h in each}
    for h in each:
        up_finish(h, mids[h])
    late[2].wait()
    downs = {h: down_start(h) for h in each}
    for h in each:
        down_finish(h, downs[h])
    for h in each:
        out[h * rh : (h + 1) * rh, :] = (residuals[h] + tp_total("t1", h, tpb)).astype(BF16)
    rest = pl.ds(1, half - 1)
    drain(gotq.at[others], flag("q"))
    drain(gotx.at[others], flag("x"))
    drain(qall.at[others], flag("g"))
    drain(gotm.at[:, others], flag("m"))
    drain(allatt.at[:, others], flag("a"))
    drain(tpa.at[:, pl.ds(1, t - 1)], flag("t0"))
    drain(upsend, flag("y"))
    drain(sqgot.at[:, others], flag("s"))
    drain(upgot2.at[:, rest], flag("z"))
    drain(upgot2.at[:, rest], flag("along"))
    drain(upgot, flag("across"))
    drain(tpb.at[:, pl.ds(1, t - 1)], flag("t1"))


def shards(
    n, t, tokens, mix_gain, w_query, w_key, w_value, w_forget, query_gain,
    key_cache, value_cache, decay_cache, w_out, mlp_gain, w_up, w_down,
):
    rows, dl = tokens.shape
    d = dl * n
    rc = rows // n
    heads = w_forget.shape[1]
    groups = key_cache.shape[1]
    sharing = heads // groups
    nq, nk = w_query.shape[1], w_key.shape[1]
    span = key_cache.shape[3]
    gd = groups * HEAD_DIM
    ffc = w_up.shape[1] // n
    half = n // 2
    parts = 2 if (rows // n) % (2 * (DEPTH // gd)) == 0 else 1
    rh = rows // parts
    rb = rh // n
    lines = rb * heads
    vmem = pl.BlockSpec(memory_space=pltpu.VMEM)
    anywhere = pl.BlockSpec(memory_space=pl.ANY)
    dma = pltpu.SemaphoreType.DMA
    return pl.pallas_call(
        functools.partial(layer_kernel, n, t, d, sharing, parts),
        out_shape=jax.ShapeDtypeStruct((rows, dl), BF16),
        in_specs=[vmem] * 3 + [anywhere] * 11,
        out_specs=vmem,
        scratch_shapes=[
            pltpu.VMEM(tokens.shape, BF16),
            pltpu.VMEM(w_query.shape, BF16),
            pltpu.VMEM(w_key.shape, BF16),
            pltpu.VMEM(w_value.shape, BF16),
            pltpu.VMEM((heads, dl), BF16),
            pltpu.VMEM((rows * gd, span), BF16),
            pltpu.VMEM((rows * gd, span), BF16),
            pltpu.VMEM((rows * heads, span), F32),
            pltpu.VMEM(w_out.shape, BF16),
            pltpu.VMEM(w_up.shape, BF16),
            pltpu.VMEM(w_down.shape, BF16),
            pltpu.VMEM((n, rc, nq + 128), F32),
            pltpu.VMEM((n, rc, 2 * nk), F32),
            pltpu.VMEM((n, rc, nq + 128), F32),
            pltpu.VMEM((n, rc, 2 * nk), F32),
            pltpu.VMEM((rc * sharing, gd), F32),
            pltpu.VMEM((n, parts, rb * sharing, gd), BF16),
            pltpu.VMEM((rc * heads, 128), F32),
            pltpu.VMEM((parts, n, lines, 128), BF16),
            pltpu.VMEM((parts, n, lines, 128), BF16),
            pltpu.VMEM((parts, lines, HEAD_DIM), F32),
            pltpu.VMEM((parts, rb, nq), BF16),
            pltpu.VMEM((parts, n, rb, nq), BF16),
            pltpu.VMEM((parts, rh, nq), F32),
            pltpu.VMEM((parts, t, rh, dl), BF16),
            pltpu.VMEM((parts, t, rh, dl), BF16),
            pltpu.VMEM((parts, half, rh, ffc), BF16),
            pltpu.VMEM((parts, half, rh, ffc), BF16),
            pltpu.VMEM((parts, half, rh, ffc), BF16),
            pltpu.VMEM((parts, half, rh, ffc), BF16),
            pltpu.VMEM((parts, half, rh, ffc), F32),
            pltpu.VMEM((parts, 8, rh), F32),
            pltpu.VMEM((parts, n, 8, rh), F32),
            pltpu.VMEM((parts, n, rh, ffc), BF16),
            dma((semaphores(n, parts)[1],)),
        ],
        compiler_params=pltpu.CompilerParams(
            collective_id=0, has_side_effects=True, vmem_limit_bytes=60 * 2**20
        ),
    )(
        mix_gain[None, :], query_gain[None, :], mlp_gain[None, :],
        tokens, w_query, w_key, w_value, w_forget.T,
        key_cache.reshape(rows * gd, span),
        value_cache.reshape(rows * gd, span),
        decay_cache.reshape(rows * heads, span),
        w_out, w_up, w_down,
    )


def solution(mesh):
    in_specs = (
        P(None, "kv"),
        P("kv"),
        P("kv", "tp"),
        P("kv", "tp"),
        P("kv", "tp"),
        P("kv", "tp"),
        P(),
        P(None, "tp", None, "kv"),
        P(None, "tp", None, "kv"),
        P(None, "tp", "kv"),
        P("tp", "kv"),
        P("kv"),
        P("kv", "tp"),
        P("tp", "kv"),
    )
    body = functools.partial(shards, mesh.shape["kv"], mesh.shape["tp"])
    return jax.shard_map(
        body, mesh=mesh, in_specs=in_specs, out_specs=P(None, "kv"), check_vma=False
    )
```

time: 68.4 us -> 64 us (0.936); the launches traced: 67.4 us -> 63.9 us
  Pallas kernels: 66 us -> 62.4 us
    pallas_call x1, Pallas kernels: 66 us -> 62.4 us  [shards(): pl.pallas_call(functools.partial(layer_kernel, n, t, d, sharing, parts),...]
where the time goes in v2:
time: 64 us; the launch traced here: 63.9 us
  Pallas kernels  62.4 us (98%)
  local copies, waits for them, and re-layouts  1.47 us (2%)
    pallas_call x1, Pallas kernels, shards(): pl.pallas_call(functools.partial(layer_kernel, n, t, d, sharing, parts),...  62.4 us
    unnamed x1, local copies, waits for them, and re-layouts  1.47 us

profile of v2, /device:TPU:0, one launch (start us, length us, event | category | flops | bytes accessed | tf_op | source)
XLA Modules:
  0.0 63.9 jit_solution(10833782952017167840)
XLA Ops:
  0.0 62.4 %shard_map.136 = bf16[64,512]{1,0:T(8,128)(2,1)} custom-call(f32[1,512]{1,0:T(1,128)} %bitcast.11, f32[1,64]{1,0:T(1,128)} %bitcast.13, f32[1,512]{1,0:T(1,128)} %bitcast.12, bf16[64,512]{1,0:T(8,128)(2,1)} %tok_hbm.1, bf16[512,512]{1,0:T(8,128)(2,1)} %wq_hbm.1, bf16[512,128]{1,0:T(8,128)(2,1)} %wk_hbm.1, bf16[512,128]{1,0:T(8,128)(2,1)} %wv_hbm.1, ...), custom_call_target="tpu_custom_call" | custom-call | tf_op jit(solution)/shard_map/pallas_call | solution.py:472
  62.4 1.5 %copy.16 = bf16[64,512]{1,0:T(8,128)(2,1)} copy(bf16[64,512]{1,0:T(8,128)(2,1)} %shard_map.136) | data formatting | bytes 131072

commit v3 on v2

--- a/solution.py
+++ b/solution.py
@@ -11,6 +11,7 @@
 HEAD_DIM = 64
 EPS = 1e-06
 DEPTH = 256
+PARTS = 2
 F32 = jnp.float32
 BF16 = jnp.bfloat16
 
@@ -27,6 +28,15 @@
             barrier, inc=1, device_id=(kv, lax.rem(tp + i, t)), device_id_type=MESH
         )
     pl.semaphore_wait(barrier, n + t - 2)
+
+
+def flip(x, m):
+    bit, y = 1, x
+    while bit <= m:
+        if m & bit:
+            y = y + bit - 2 * bit * lax.rem(x // bit, 2)
+        bit *= 2
+    return y
 
 
 def remote(src, dst, send, recv, kv, tp):
@@ -43,7 +53,7 @@
 def semaphores(n, parts):
     half = n // 2
     sizes = dict(
-        first=5, late=3, cache=3 * parts, q=2, x=2, g=2, m=1 + parts, a=1 + parts,
+        first=5, late=3, cache=3 * parts, q=2, e=2, x=2, g=2, m=1 + parts, a=1 + parts,
         t0=1 + parts, t1=1 + parts, y=1 + parts * half, s=1 + parts, z=1 + parts,
         along=1 + parts * half, across=1 + parts * half,
     )
@@ -64,9 +74,9 @@
     mgain, qgain, pgain, tok_hbm, wq_hbm, wk_hbm, wv_hbm, wf_hbm,
     k_hbm, v_hbm, d_hbm, wo_hbm, wu_hbm, wd_hbm, out,
     tok, wq, wk, wv, wf, kbuf, vbuf, dbuf, wo, wu, wd,
-    partq, partx, gotq, gotx, qs, qall, own, msg, gotm, heads_s,
+    stage_q, parts_s, got_s, partq, partx, gotq, gotx, qs, qall, own, msg, gotm, heads_s,
     att, allatt, full, tpa, tpb, upsend, upgot, upsend2, upgot2, keep, sqs, sqgot, hid,
-    sem,
+    w_a, w_b, stat_a, stat_b, sem,
 ):
     kv, tp = lax.axis_index("kv"), lax.axis_index("tp")
     rows, dl = tok.shape
@@ -93,7 +103,7 @@
         pltpu.make_async_copy(ref, ref, s).wait()
 
     def block_of(i):
-        return lax.rem(kv + i, n)
+        return flip(kv, i)
 
     first = [
         local(a, b, flag("first", j))
@@ -128,8 +138,8 @@
         remote(src, dst, flag(name), flag(name, 1 + slot), peer, tp).start()
 
     def to_all(name, src, dst, slot=0):
-        for i in range(1, n):
-            peer = lax.rem(kv + i, n)
+        for i in range(n - 1, 0, -1):
+            peer = block_of(i)
             send(name, src(peer), dst(i), peer, slot)
 
     for c in first:
@@ -147,10 +157,12 @@
         for h in range(parts)
     ]
     for p, to, cut in pieces:
-        partq[p, to, 0:nq] = q[cut]
-        partq[p, to, nq : nq + 128] = jnp.broadcast_to(squares[cut], (rb, 128))
-        partq[p, to, nq : nq + heads] = f[cut]
+        stage_q[p, to, :] = q[cut]
+        parts_s[p, to, :] = jnp.broadcast_to(squares[cut], (rb, 128))
+        parts_s[p, to, 0:heads] = f[cut]
+    partq[...] = stage_q[...].astype(BF16)
     to_all("q", lambda p: partq.at[p], lambda i: gotq.at[i])
+    to_all("e", lambda p: parts_s.at[p], lambda i: got_s.at[i])
     k = jnp.dot(normed, wk[...], preferred_element_type=F32)
     v = jnp.dot(normed, wv[...], preferred_element_type=F32)
     for p, to, cut in pieces:
@@ -158,14 +170,16 @@
         partx[p, to, nk : 2 * nk] = v[cut]
     to_all("x", lambda p: partx.at[p], lambda i: gotx.at[i])
 
-    total = partq[kv]
+    total, stats = stage_q[kv], parts_s[kv]
     others = pl.ds(1, n - 1)
     drain(gotq.at[others], flag("q", 1))
+    drain(got_s.at[others], flag("e", 1))
     for i in range(1, n):
-        total = total + gotq[i]
-    scale = lax.rsqrt(total[:, nq + 127 : nq + 128] / d + EPS)
-    raw = total[:, 0:nq] * scale
-    gate = total[:, nq : nq + heads] * scale
+        total = total + gotq[i].astype(F32)
+        stats = stats + got_s[i]
+    scale = lax.rsqrt(stats[:, 127:128] / d + EPS)
+    raw = total * scale
+    gate = stats[:, 0:heads] * scale
     forget = jnp.minimum(gate, 0.0) - jnp.log1p(jnp.exp(-jnp.abs(gate)))
     queries = []
     for h in range(heads):
@@ -202,12 +216,21 @@
 
     group_row = lax.broadcasted_iota(jnp.int32, (heads, gd), 0) // sharing
     group_lane = lax.broadcasted_iota(jnp.int32, (heads, gd), 1) // HEAD_DIM
-    slot = lax.broadcasted_iota(jnp.int32, (tile, HEAD_DIM), 0) // sharing
+    slot = lax.broadcasted_iota(jnp.int32, (HEAD_DIM, lines), 1) // sharing
     lane = lax.broadcasted_iota(jnp.int32, (tile, HEAD_DIM), 1) // 16
 
-    def attend(h, bs):
-        todo = [(b, s) for b in bs for s in range(lines // tile)]
-        scores, sums, peaks = [], [], []
+    steps = lines // tile
+    many = max(1, 4 // steps) if parts > 1 else 2
+    turns = n // many
+
+    def blocks_at(u):
+        at = (u % turns) * many
+        return u // turns, [n - 1 - at - e for e in range(many)]
+
+    def weigh(u, w_s, stat_s):
+        h, peers = blocks_at(u)
+        todo = [(block_of(i), s) for i in peers for s in range(steps)]
+        scores = []
         for b, s in todo:
             qt = qall[b, h].astype(F32)
             strips = []
@@ -227,52 +250,46 @@
                 jnp.dot(left, kbuf[at, :], preferred_element_type=F32) * (HEAD_DIM**-0.5)
                 + dbuf[lt, :]
             )
-        weights = []
-        for sc in scores:
+        for m, sc in enumerate(scores):
             hi, lo = split(jnp.max(sc, axis=1, keepdims=True))
             w = jnp.exp(sc - (hi + lo))
-            peaks.append((hi, lo))
-            sums.append(split(jnp.sum(w, axis=1, keepdims=True)))
-            weights.append(w.astype(BF16))
-        for (b, s), w, top, mass in zip(todo, weights, peaks, sums):
-            row = h * rh + b * rb + s * pack
-            at = pl.ds(pl.multiple_of(row * gd, DEPTH), DEPTH)
+            mass = split(jnp.sum(w, axis=1, keepdims=True))
+            w_s[m * tile : (m + 1) * tile, :] = w.astype(BF16)
+            stat_s[m * tile : (m + 1) * tile, :] = jnp.where(
+                lane == 0,
+                hi,
+                jnp.where(lane == 1, lo, jnp.where(lane == 2, mass[0], mass[1])),
+            )
+
+    def gather_values(u, w_s, stat_s):
+        h, peers = blocks_at(u)
+        for m, i in enumerate(peers):
+            b = block_of(i)
+            at = pl.ds(pl.multiple_of((h * rh + b * rb) * gd, rb * gd), rb * gd)
+            mine = slice(m * lines, (m + 1) * lines)
             o = lax.dot_general(
-                w, vbuf[at, :], (((1,), (1,)), ((), ())), preferred_element_type=F32
+                vbuf[at, :], w_s[mine, :], (((1,), (1,)), ((), ())),
+                preferred_element_type=F32,
             )
-            picked = o[:, 0:HEAD_DIM]
-            for g in range(1, DEPTH // HEAD_DIM):
-                picked = jnp.where(slot == g, o[:, g * HEAD_DIM : (g + 1) * HEAD_DIM], picked)
-            stats = jnp.where(
-                lane == 0,
-                top[0],
-                jnp.where(lane == 1, top[1], jnp.where(lane == 2, mass[0], mass[1])),
-            )
-            msg[h, b, s * tile : (s + 1) * tile, :] = jnp.concatenate(
-                [picked, stats], axis=1
-            ).astype(BF16)
-
-    twin = n // 2
-
-    def step(u, h):
-        i0 = 1 + 2 * u
-        i1 = lax.rem(i0 + 1, n)
-        attend(h, [block_of(i0), block_of(i1)])
-
-        def message(i):
-            b = block_of(i)
-            send("m", msg.at[h, b], gotm.at[h, i], b, h)
-
-        message(i0)
-
-        @pl.when(i1 != 0)
-        def _():
-            message(i1)
-
-        return h
-
-    def attend_half(h, start, stop):
-        lax.fori_loop(start, stop, lambda u, carry: step(u, h) * 0, 0)
+            picked = o[0:HEAD_DIM]
+            for g in range(1, rb * groups):
+                picked = jnp.where(slot == g, o[g * HEAD_DIM : (g + 1) * HEAD_DIM], picked)
+            msg[h, b] = jnp.concatenate([picked.T, stat_s[mine, :]], axis=1).astype(BF16)
+
+    def message(u):
+        h, peers = blocks_at(u)
+        for i in peers:
+            if i:
+                b = block_of(i)
+                send("m", msg.at[h, b], gotm.at[h, i], b, h)
+
+    slots = (w_a, stat_a), (w_b, stat_b)
+
+    def attend(u):
+        if u + 1 < parts * turns:
+            weigh(u + 1, *slots[(u + 1) % 2])
+        gather_values(u, *slots[u % 2])
+        message(u)
 
     def combine(h):
         extra = own[h * lines : (h + 1) * lines, :]
@@ -326,7 +343,10 @@
     side = lax.rem(kv, 2)
     place = kv // 2
     partner = kv + 1 - 2 * side
-    order = list(range(1, half)) + [0]
+    order = list(range(half - 1, -1, -1))
+
+    def across_z(j):
+        return 2 * flip(place, j)
 
     def up_start(h):
         attn = tp_total("t0", h, tpa)
@@ -338,10 +358,10 @@
             return jnp.dot(normed, wu[:, cols], preferred_element_type=F32)
 
         for j in order:
-            upsend[h, j] = term(2 * lax.rem(place + j, half) + 1 - side).astype(BF16)
+            upsend[h, j] = term(across_z(j) + 1 - side).astype(BF16)
             send("y", upsend.at[h, j], upgot.at[h, j], partner, h * half + j)
         for j in order:
-            keep[h, j] = term(2 * lax.rem(place + j, half) + side)
+            keep[h, j] = term(across_z(j) + side)
         sqs[h] = lax.dot_general(
             jnp.ones((8, dl), F32),
             residual * residual,
@@ -358,10 +378,7 @@
             part = keep[h, j] + upgot[h, j].astype(F32)
             if j:
                 upsend2[h, j] = part.astype(BF16)
-                send(
-                    "z", upsend2.at[h, j], upgot2.at[h, j],
-                    2 * lax.rem(place + j, half) + side, h,
-                )
+                send("z", upsend2.at[h, j], upgot2.at[h, j], across_z(j) + side, h)
         return part
 
     def up_finish(h, part):
@@ -380,8 +397,8 @@
         hid[h, kv] = jnp.square(jnp.maximum(part * scale, 0.0)).astype(BF16)
         mine = hid.at[h, kv]
         send("across", mine, mine, partner, h * half)
-        for j in range(1, half):
-            send("along", mine, mine, 2 * lax.rem(place + j, half) + side, h * half + j)
+        for j in order[:-1]:
+            send("along", mine, mine, across_z(j) + side, h * half + j)
 
     def lower(h, src):
         there = pl.ds(pl.multiple_of(src * ffc, ffc), ffc)
@@ -389,8 +406,8 @@
 
     def down_start(h):
         down = lower(h, kv)
-        for j in range(1, half):
-            src = 2 * lax.rem(place + half - j, half) + side
+        for j in order[:-1]:
+            src = across_z(j) + side
             block = hid.at[h, src]
             drain(block, flag("along", 1 + h * half + j))
             send("across", block, block, partner, h * half + j)
@@ -399,41 +416,65 @@
 
     def down_finish(h, down):
         for j in range(half):
-            src = 2 * lax.rem(place + half - j, half) + 1 - side
+            src = across_z(j) + 1 - side
             drain(hid.at[h, src], flag("across", 1 + h * half + j))
             down = down + lower(h, src)
         tp_send("t1", h, tpb, down)
 
-    each = range(parts)
-    last = parts - 1
+    residuals, kept, downs = {}, {}, {}
+
+    def stage_1(h):
+        if h == 0:
+            late[0].wait()
+        project_out(h)
+
+    def stage_2(h):
+        if h == 0:
+            late[1].wait()
+        residuals[h] = up_start(h)
+
+    def stage_3(h):
+        kept[h] = up_middle(h)
+
+    def stage_4(h):
+        up_finish(h, kept[h])
+
+    def stage_5(h):
+        if h == 0:
+            late[2].wait()
+        downs[h] = down_start(h)
+
+    def stage_6(h):
+        down_finish(h, downs[h])
+
+    def stage_7(h):
+        out[h * rh : (h + 1) * rh, :] = (residuals[h] + tp_total("t1", h, tpb)).astype(BF16)
+
+    stages = (combine, stage_1, stage_2, stage_3, stage_4, stage_5, stage_6, stage_7)
+    share = 1.0 / parts
+    gaps = (
+        3.3, 4.5, 2.2 + 2.8 * share, 2.2 + 5.6 * share, 3.5, 3.6 + 2.8 * share,
+        2.2 + 1.5 * share, 2.2 + 2.8 * share,
+    )
+    pace = 4.0 / (parts * turns)
+    events = [(u * pace, 0, functools.partial(attend, u)) for u in range(parts * turns)]
+    for h in range(parts):
+        when = (h + 1) * turns * pace
+        for stage, gap in zip(stages, gaps):
+            when += gap
+            events.append((when, 1 + h, functools.partial(stage, h)))
+    events.sort(key=lambda e: e[:2])
+
     drain(qall.at[others], flag("g", 1))
-    for h in each:
+    for h in range(parts):
         for c in cache_loads(h):
             c.wait()
-        if h < last or parts == 1:
-            attend_half(h, 0, twin)
-        else:
-            attend_half(h, 0, twin // 2)
-            for e in range(last):
-                combine(e)
-            attend_half(h, twin // 2, twin)
-    combine(last)
-    late[0].wait()
-    for h in each:
-        project_out(h)
-    late[1].wait()
-    residuals = {h: up_start(h) for h in each}
-    mids = {h: up_middle(h) for h in each}
-    for h in each:
-        up_finish(h, mids[h])
-    late[2].wait()
-    downs = {h: down_start(h) for h in each}
-    for h in each:
-        down_finish(h, downs[h])
-    for h in each:
-        out[h * rh : (h + 1) * rh, :] = (residuals[h] + tp_total("t1", h, tpb)).astype(BF16)
+    weigh(0, *slots[0])
+    for _, _, event in events:
+        event()
     rest = pl.ds(1, half - 1)
     drain(gotq.at[others], flag("q"))
+    drain(got_s.at[others], flag("e"))
     drain(gotx.at[others], flag("x"))
     drain(qall.at[others], flag("g"))
     drain(gotm.at[:, others], flag("m"))
@@ -462,9 +503,11 @@
     gd = groups * HEAD_DIM
     ffc = w_up.shape[1] // n
     half = n // 2
-    parts = 2 if (rows // n) % (2 * (DEPTH // gd)) == 0 else 1
+    pack = DEPTH // gd
+    parts = PARTS if (rows // n) % (PARTS * pack) == 0 else 1
     rh = rows // parts
     rb = rh // n
+    many = max(1, 4 // (rb // pack)) if parts > 1 else 2
     lines = rb * heads
     vmem = pl.BlockSpec(memory_space=pltpu.VMEM)
     anywhere = pl.BlockSpec(memory_space=pl.ANY)
@@ -486,9 +529,12 @@
             pltpu.VMEM(w_out.shape, BF16),
             pltpu.VMEM(w_up.shape, BF16),
             pltpu.VMEM(w_down.shape, BF16),
-            pltpu.VMEM((n, rc, nq + 128), F32),
+            pltpu.VMEM((n, rc, nq), F32),
+            pltpu.VMEM((n, rc, 128), F32),
+            pltpu.VMEM((n, rc, 128), F32),
+            pltpu.VMEM((n, rc, nq), BF16),
             pltpu.VMEM((n, rc, 2 * nk), F32),
-            pltpu.VMEM((n, rc, nq + 128), F32),
+            pltpu.VMEM((n, rc, nq), BF16),
             pltpu.VMEM((n, rc, 2 * nk), F32),
             pltpu.VMEM((rc * sharing, gd), F32),
             pltpu.VMEM((n, parts, rb * sharing, gd), BF16),
@@ -509,6 +555,10 @@
             pltpu.VMEM((parts, 8, rh), F32),
             pltpu.VMEM((parts, n, 8, rh), F32),
             pltpu.VMEM((parts, n, rh, ffc), BF16),
+            pltpu.VMEM((many * lines, span), BF16),
+            pltpu.VMEM((many * lines, span), BF16),
+            pltpu.VMEM((many * lines, HEAD_DIM), F32),
+            pltpu.VMEM((many * lines, HEAD_DIM), F32),
             dma((semaphores(n, parts)[1],)),
         ],
         compiler_params=pltpu.CompilerParams(

time: 64 us -> 58.7 us (0.917)
  Pallas kernels: 62.4 us -> 57.1 us
    pallas_call x1, Pallas kernels: 62.4 us -> 57.1 us  [shards(): pl.pallas_call(functools.partial(layer_kernel, n, t, d, sharing, parts),...]
where the time goes in v3:
time: 58.7 us; the launch traced here: 58.6 us
  Pallas kernels  57.1 us (97%)
  local copies, waits for them, and re-layouts  1.47 us (3%)
    pallas_call x1, Pallas kernels, shards(): pl.pallas_call(functools.partial(layer_kernel, n, t, d, sharing, parts),...  57.1 us
    unnamed x1, local copies, waits for them, and re-layouts  1.47 us

profile of v3, /device:TPU:0, one launch (start us, length us, event | category | flops | bytes accessed | tf_op | source)
XLA Modules:
  0.0 58.6 jit_solution(8452881166627585155)
XLA Ops:
  0.0 57.1 %shard_map.136 = bf16[64,512]{1,0:T(8,128)(2,1)} custom-call(f32[1,512]{1,0:T(1,128)} %bitcast.11, f32[1,64]{1,0:T(1,128)} %bitcast.13, f32[1,512]{1,0:T(1,128)} %bitcast.12, bf16[64,512]{1,0:T(8,128)(2,1)} %tok_hbm.1, bf16[512,512]{1,0:T(8,128)(2,1)} %wq_hbm.1, bf16[512,128]{1,0:T(8,128)(2,1)} %wk_hbm.1, bf16[512,128]{1,0:T(8,128)(2,1)} %wv_hbm.1, ...), custom_call_target="tpu_custom_call" | custom-call | tf_op jit(solution)/shard_map/pallas_call | solution.py:515
  57.1 1.5 %copy.16 = bf16[64,512]{1,0:T(8,128)(2,1)} copy(bf16[64,512]{1,0:T(8,128)(2,1)} %shard_map.136) | data formatting | bytes 131072

commit v4 on v3

--- a/solution.py
+++ b/solution.py
@@ -53,7 +53,7 @@
 def semaphores(n, parts):
     half = n // 2
     sizes = dict(
-        first=5, late=3, cache=3 * parts, q=2, e=2, x=2, g=2, m=1 + parts, a=1 + parts,
+        first=5, late=3, cache=3 * half, q=2, e=2, x=2, g=1 + n, m=1 + parts, a=1 + parts,
         t0=1 + parts, t1=1 + parts, y=1 + parts * half, s=1 + parts, z=1 + parts,
         along=1 + parts * half, across=1 + parts * half,
     )
@@ -114,17 +114,21 @@
     for c in first:
         c.start()
 
-    def cache_loads(h):
-        at = pl.ds(h * rh * gd, rh * gd)
-        lt = pl.ds(h * rh * heads, rh * heads)
-        return (
-            local(k_hbm.at[at], kbuf.at[at], flag("cache", 3 * h)),
-            local(d_hbm.at[lt], dbuf.at[lt], flag("cache", 3 * h + 1)),
-            local(v_hbm.at[at], vbuf.at[at], flag("cache", 3 * h + 2)),
-        )
-
-    for h in range(parts):
-        for c in cache_loads(h):
+    half = n // 2
+    side = lax.rem(kv, 2)
+    place = kv // 2
+    partner = kv + 1 - 2 * side
+
+    def cache_loads(j):
+        z = flip(place, j)
+        return [
+            local(a.at[:, z], b.at[:, z], flag("cache", 3 * j + m))
+            for m, (a, b) in enumerate(((k_hbm, kbuf), (d_hbm, dbuf), (v_hbm, vbuf)))
+        ]
+
+    near = [0, 1] + list(range(half - 1, 1, -1))
+    for j in near:
+        for c in cache_loads(j):
             c.start()
     late = [
         local(a, b, flag("late", j))
@@ -194,44 +198,27 @@
         )
     for h in range(parts):
         qall[kv, h] = qs[h * rb * sharing : (h + 1) * rb * sharing, :].astype(BF16)
-    to_all("g", lambda p: qall.at[kv], lambda i: qall.at[kv])
-    extra = partx[kv]
-    drain(gotx.at[others], flag("x", 1))
-    for i in range(1, n):
-        extra = extra + gotx[i]
-    extra = (extra * scale).astype(BF16).astype(F32)
-    for h in range(heads):
-        g = h // sharing
-        key = extra[:, g * HEAD_DIM : (g + 1) * HEAD_DIM]
-        value = extra[:, nk + g * HEAD_DIM : nk + (g + 1) * HEAD_DIM]
-        score = jnp.sum(queries[h] * key, axis=1, keepdims=True) * (HEAD_DIM**-0.5)
-        own[pl.ds(h, rc, stride=heads), :] = jnp.concatenate(
-            [
-                value,
-                jnp.broadcast_to(score, (rc, 32)),
-                jnp.broadcast_to(forget[:, h : h + 1], (rc, 32)),
-            ],
-            axis=1,
-        )
-
+    for i in range(n - 1, 0, -1):
+        send("g", qall.at[kv], qall.at[kv], block_of(i), i)
     group_row = lax.broadcasted_iota(jnp.int32, (heads, gd), 0) // sharing
     group_lane = lax.broadcasted_iota(jnp.int32, (heads, gd), 1) // HEAD_DIM
     slot = lax.broadcasted_iota(jnp.int32, (HEAD_DIM, lines), 1) // sharing
     lane = lax.broadcasted_iota(jnp.int32, (tile, HEAD_DIM), 1) // 16
 
     steps = lines // tile
-    many = max(1, 4 // steps) if parts > 1 else 2
-    turns = n // many
-
-    def blocks_at(u):
-        at = (u % turns) * many
-        return u // turns, [n - 1 - at - e for e in range(many)]
+    if parts == 2 and half > 2:
+        far = [2 * j for j in near[2:]]
+        ends = [[(m + 1, h), (m, h)] for h in range(2) for m in far]
+        walk = [[(0, 0), (0, 1)], [(1, 0), (1, 1)]]
+        walk += [[(3, 0), (2, 0)]] + ends[:len(far)] + ends[len(far):] + [[(3, 1), (2, 1)]]
+    else:
+        walk = [[(2 * j + 1, h), (2 * j, h)] for h in range(parts) for j in near]
 
     def weigh(u, w_s, stat_s):
-        h, peers = blocks_at(u)
-        todo = [(block_of(i), s) for i in peers for s in range(steps)]
+        todo = [(i, h, s) for i, h in walk[u] for s in range(steps)]
         scores = []
-        for b, s in todo:
+        for i, h, s in todo:
+            b = block_of(i)
             qt = qall[b, h].astype(F32)
             strips = []
             for j in range(pack):
@@ -243,12 +230,13 @@
                     jnp.concatenate([one if m == j else zero for m in range(pack)], axis=1)
                 )
             left = jnp.concatenate(strips, axis=0).astype(BF16)
-            row = h * rh + b * rb + s * pack
-            at = pl.ds(pl.multiple_of(row * gd, DEPTH), DEPTH)
-            lt = pl.ds(pl.multiple_of(row * heads, tile), tile)
+            low = lax.rem(b, 2)
+            at = pl.ds(pl.multiple_of(low * rb * gd + s * DEPTH, DEPTH), DEPTH)
+            lt = pl.ds(pl.multiple_of(low * lines + s * tile, tile), tile)
             scores.append(
-                jnp.dot(left, kbuf[at, :], preferred_element_type=F32) * (HEAD_DIM**-0.5)
-                + dbuf[lt, :]
+                jnp.dot(left, kbuf[h, b // 2, at, :], preferred_element_type=F32)
+                * (HEAD_DIM**-0.5)
+                + dbuf[h, b // 2, lt, :]
             )
         for m, sc in enumerate(scores):
             hi, lo = split(jnp.max(sc, axis=1, keepdims=True))
@@ -262,13 +250,12 @@
             )
 
     def gather_values(u, w_s, stat_s):
-        h, peers = blocks_at(u)
-        for m, i in enumerate(peers):
+        for m, (i, h) in enumerate(walk[u]):
             b = block_of(i)
-            at = pl.ds(pl.multiple_of((h * rh + b * rb) * gd, rb * gd), rb * gd)
+            at = pl.ds(pl.multiple_of(lax.rem(b, 2) * rb * gd, rb * gd), rb * gd)
             mine = slice(m * lines, (m + 1) * lines)
             o = lax.dot_general(
-                vbuf[at, :], w_s[mine, :], (((1,), (1,)), ((), ())),
+                vbuf[h, b // 2, at, :], w_s[mine, :], (((1,), (1,)), ((), ())),
                 preferred_element_type=F32,
             )
             picked = o[0:HEAD_DIM]
@@ -277,19 +264,55 @@
             msg[h, b] = jnp.concatenate([picked.T, stat_s[mine, :]], axis=1).astype(BF16)
 
     def message(u):
-        h, peers = blocks_at(u)
-        for i in peers:
+        for i, h in walk[u]:
             if i:
                 b = block_of(i)
                 send("m", msg.at[h, b], gotm.at[h, i], b, h)
 
     slots = (w_a, stat_a), (w_b, stat_b)
 
+    seen, loaded = set(), set()
+
+    def ready(u):
+        for i, h in walk[u]:
+            if i and i not in seen:
+                drain(qall.at[block_of(i)], flag("g", 1 + i))
+            seen.add(i)
+            if i // 2 not in loaded:
+                for c in cache_loads(i // 2):
+                    c.wait()
+            loaded.add(i // 2)
+
     def attend(u):
-        if u + 1 < parts * turns:
+        if u == 0:
+            gather_values(u, *slots[0])
+            own_terms()
+        if u + 1 < len(walk):
+            ready(u + 1)
             weigh(u + 1, *slots[(u + 1) % 2])
-        gather_values(u, *slots[u % 2])
+        if u:
+            gather_values(u, *slots[u % 2])
         message(u)
+
+    def own_terms():
+        extra = partx[kv]
+        drain(gotx.at[others], flag("x", 1))
+        for i in range(1, n):
+            extra = extra + gotx[i]
+        extra = (extra * scale).astype(BF16).astype(F32)
+        for h in range(heads):
+            g = h // sharing
+            key = extra[:, g * HEAD_DIM : (g + 1) * HEAD_DIM]
+            value = extra[:, nk + g * HEAD_DIM : nk + (g + 1) * HEAD_DIM]
+            score = jnp.sum(queries[h] * key, axis=1, keepdims=True) * (HEAD_DIM**-0.5)
+            own[pl.ds(h, rc, stride=heads), :] = jnp.concatenate(
+                [
+                    value,
+                    jnp.broadcast_to(score, (rc, 32)),
+                    jnp.broadcast_to(forget[:, h : h + 1], (rc, 32)),
+                ],
+                axis=1,
+            )
 
     def combine(h):
         extra = own[h * lines : (h + 1) * lines, :]
@@ -339,10 +362,6 @@
         attn = jnp.dot(full[h].astype(BF16), wo[...], preferred_element_type=F32)
         tp_send("t0", h, tpa, attn)
 
-    half = n // 2
-    side = lax.rem(kv, 2)
-    place = kv // 2
-    partner = kv + 1 - 2 * side
     order = list(range(half - 1, -1, -1))
 
     def across_z(j):
@@ -451,27 +470,13 @@
         out[h * rh : (h + 1) * rh, :] = (residuals[h] + tp_total("t1", h, tpb)).astype(BF16)
 
     stages = (combine, stage_1, stage_2, stage_3, stage_4, stage_5, stage_6, stage_7)
-    share = 1.0 / parts
-    gaps = (
-        3.3, 4.5, 2.2 + 2.8 * share, 2.2 + 5.6 * share, 3.5, 3.6 + 2.8 * share,
-        2.2 + 1.5 * share, 2.2 + 2.8 * share,
-    )
-    pace = 4.0 / (parts * turns)
-    events = [(u * pace, 0, functools.partial(attend, u)) for u in range(parts * turns)]
-    for h in range(parts):
-        when = (h + 1) * turns * pace
-        for stage, gap in zip(stages, gaps):
-            when += gap
-            events.append((when, 1 + h, functools.partial(stage, h)))
-    events.sort(key=lambda e: e[:2])
-
-    drain(qall.at[others], flag("g", 1))
-    for h in range(parts):
-        for c in cache_loads(h):
-            c.wait()
+    ready(0)
     weigh(0, *slots[0])
-    for _, _, event in events:
-        event()
+    for u in range(len(walk)):
+        attend(u)
+    for stage in stages:
+        for h in range(parts):
+            stage(h)
     rest = pl.ds(1, half - 1)
     drain(gotq.at[others], flag("q"))
     drain(got_s.at[others], flag("e"))
@@ -507,7 +512,6 @@
     parts = PARTS if (rows // n) % (PARTS * pack) == 0 else 1
     rh = rows // parts
     rb = rh // n
-    many = max(1, 4 // (rb // pack)) if parts > 1 else 2
     lines = rb * heads
     vmem = pl.BlockSpec(memory_space=pltpu.VMEM)
     anywhere = pl.BlockSpec(memory_space=pl.ANY)
@@ -523,9 +527,9 @@
             pltpu.VMEM(w_key.shape, BF16),
             pltpu.VMEM(w_value.shape, BF16),
             pltpu.VMEM((heads, dl), BF16),
-            pltpu.VMEM((rows * gd, span), BF16),
-            pltpu.VMEM((rows * gd, span), BF16),
-            pltpu.VMEM((rows * heads, span), F32),
+            pltpu.VMEM((parts, half, 2 * rb * gd, span), BF16),
+            pltpu.VMEM((parts, half, 2 * rb * gd, span), BF16),
+            pltpu.VMEM((parts, half, 2 * lines, span), F32),
             pltpu.VMEM(w_out.shape, BF16),
             pltpu.VMEM(w_up.shape, BF16),
             pltpu.VMEM(w_down.shape, BF16),
@@ -555,10 +559,10 @@
             pltpu.VMEM((parts, 8, rh), F32),
             pltpu.VMEM((parts, n, 8, rh), F32),
             pltpu.VMEM((parts, n, rh, ffc), BF16),
-            pltpu.VMEM((many * lines, span), BF16),
-            pltpu.VMEM((many * lines, span), BF16),
-            pltpu.VMEM((many * lines, HEAD_DIM), F32),
-            pltpu.VMEM((many * lines, HEAD_DIM), F32),
+            pltpu.VMEM((2 * lines, span), BF16),
+            pltpu.VMEM((2 * lines, span), BF16),
+            pltpu.VMEM((2 * lines, HEAD_DIM), F32),
+            pltpu.VMEM((2 * lines, HEAD_DIM), F32),
             dma((semaphores(n, parts)[1],)),
         ],
         compiler_params=pltpu.CompilerParams(
@@ -567,9 +571,9 @@
     )(
         mix_gain[None, :], query_gain[None, :], mlp_gain[None, :],
         tokens, w_query, w_key, w_value, w_forget.T,
-        key_cache.reshape(rows * gd, span),
-        value_cache.reshape(rows * gd, span),
-        decay_cache.reshape(rows * heads, span),
+        key_cache.reshape(parts, half, 2 * rb * gd, span),
+        value_cache.reshape(parts, half, 2 * rb * gd, span),
+        decay_cache.reshape(parts, half, 2 * lines, span),
         w_out, w_up, w_down,
     )
 

time: 58.7 us -> 57.4 us (0.978)
  Pallas kernels: 57.1 us -> 55.8 us
    pallas_call x1, Pallas kernels: 57.1 us -> 55.8 us  [shards(): pl.pallas_call(functools.partial(layer_kernel, n, t, d, sharing, parts),...]
where the time goes in v4:
time: 57.4 us; the launch traced here: 57.3 us
  Pallas kernels  55.8 us (97%)
  local copies, waits for them, and re-layouts  1.47 us (3%)
    pallas_call x1, Pallas kernels, shards(): pl.pallas_call(functools.partial(layer_kernel, n, t, d, sharing, parts),...  55.8 us
    unnamed x1, local copies, waits for them, and re-layouts  1.47 us

profile of v4, /device:TPU:0, one launch (start us, length us, event | category | flops | bytes accessed | tf_op | source)
XLA Modules:
  0.0 57.3 jit_solution(5100908039535320365)
XLA Ops:
  0.0 55.8 %shard_map.136 = bf16[64,512]{1,0:T(8,128)(2,1)} custom-call(f32[1,512]{1,0:T(1,128)} %bitcast.11, f32[1,64]{1,0:T(1,128)} %bitcast.13, f32[1,512]{1,0:T(1,128)} %bitcast.12, bf16[64,512]{1,0:T(8,128)(2,1)} %tok_hbm.1, bf16[512,512]{1,0:T(8,128)(2,1)} %wq_hbm.1, bf16[512,128]{1,0:T(8,128)(2,1)} %wk_hbm.1, bf16[512,128]{1,0:T(8,128)(2,1)} %wv_hbm.1, ...), custom_call_target="tpu_custom_call" | custom-call | tf_op jit(solution)/shard_map/pallas_call | solution.py:519
  55.8 1.5 %copy.16 = bf16[64,512]{1,0:T(8,128)(2,1)} copy(bf16[64,512]{1,0:T(8,128)(2,1)} %shard_map.136) | data formatting | bytes 131072
